TPU v7x, 128 devices: a whole 4x4x4 slice. The times are simulated.
128 devices in a mesh: ra: 16 (over z, y), cb: 8 (over x, core).
Axes of the slice: x: 4, y: 4, z: 4, core: 2. Of those that a mesh axis runs over, the one named last changes fastest.
Arguments:
- tokens: bfloat16 [4, 128, 4096], P(None, None, 'ra'), may hold values from -64 to 64
- norm_gain: float32 [2, 4096], P(None, 'ra'), may hold values from 0.1 to 1.9
- gate_weight: bfloat16 [2, 4096, 11264], P(None, 'ra', 'cb'), may hold values from -0.09375 to 0.09375
- up_weight: bfloat16 [2, 4096, 11264], P(None, 'ra', 'cb'), may hold values from -0.09375 to 0.09375
- gate_taps: float32 [2, 3, 11264], P(None, None, 'cb'), may hold values from -3 to 3
- up_taps: float32 [2, 3, 11264], P(None, None, 'cb'), may hold values from -3 to 3
- gate_bias: float32 [2, 11264], P(None, 'cb'), may hold values from -3 to 3
- up_bias: float32 [2, 11264], P(None, 'cb'), may hold values from -3 to 3
- down_weight: bfloat16 [2, 11264, 4096], P(None, 'cb', 'ra'), may hold values from -0.0546875 to 0.0546875
Outputs:
- mixed: bfloat16 [4, 128, 4096], P(None, None, 'ra')
All inputs are finite; a program needn't handle non-finite values.
Results may differ from a plain program's by a relative error of at most 0.03.
Values may be sent and summed in bfloat16 or wider, within the bound.
No kernel may reach another device: no remote copies, remote signals or barrier semaphores. Data moves between devices by JAX's collectives and lax.ppermute only.
A program may use at most 64 MiB of HBM per device.

v0:
```python
import jax
import jax.numpy as jnp
from jax import lax
from jax.experimental import pallas as pl
from jax.experimental.pallas import tpu as pltpu
from jax.sharding import PartitionSpec as P


D = 4096
KERNEL = 3
LAYERS = 2
SIDE = 4
EXTRA = 16
AXES = ("ra", "cb")
BF16 = jnp.bfloat16
F32 = jnp.float32

eps = 1e-06
resid_scale = 0.5


def pairs(move):
    out = []
    for z in range(SIDE):
        for y in range(SIDE):
            for x in range(SIDE):
                for core in range(2):
                    to_z, to_y, to_x, to_core = move(z, y, x, core)
                    here = ((z * SIDE + y) * SIDE + x) * 2 + core
                    there = ((to_z * SIDE + to_y) * SIDE + to_x) * 2 + to_core
                    out.append((here, there))
    return out


def to_twin(value):
    return lax.ppermute(value, AXES, pairs(lambda z, y, x, c: (z, y, x, 1 - c)))


def first_move(d):
    return lambda z, y, x, c: (z, y ^ d, x, c) if c == 1 else (z ^ d, y, x, c)


def second_move(d):
    return lambda z, y, x, c: (z ^ d, y, x, c) if c == 1 else (z, y ^ d, x, c)


def x_move(d):
    return lambda z, y, x, c: (z, y, x ^ d, c)


def moved(move, values):
    got = {}
    for d in (1, 2, 3):
        got[d] = lax.ppermute(values[d], AXES, pairs(move(d)))
    return got


VMEM = pl.BlockSpec(memory_space=pltpu.VMEM)
HBM = pl.BlockSpec(memory_space=pltpu.HBM)


def position():
    cb, ra = lax.axis_index("cb"), lax.axis_index("ra")
    core, row, col = cb & 1, ra >> 2, ra & 3
    return core, jnp.where(core == 1, col, row), jnp.where(core == 1, row, col)


def local(kernel, outs, *args, flops=10**9, specs=None, scratch=()):
    many = isinstance(outs, list)
    moved = sum(a.size * a.dtype.itemsize for a in args)
    return pl.pallas_call(
        kernel,
        in_specs=specs or [VMEM] * len(args),
        out_specs=[VMEM] * len(outs) if many else VMEM,
        out_shape=outs,
        scratch_shapes=scratch,
        compiler_params=pltpu.CompilerParams(vmem_limit_bytes=16 * 2**20),
        cost_estimate=pl.CostEstimate(flops=flops, bytes_accessed=moved, transcendentals=0),
    )(*args)


def in_hbm(value):
    return pltpu.with_memory_space_constraint(value, pltpu.HBM)


def array(shape, dtype):
    return jax.ShapeDtypeStruct(shape, dtype)


def split_rows(row_sum):
    high = row_sum.astype(BF16).astype(F32)
    low = row_sum - high
    shape = (EXTRA, row_sum.shape[1])
    row = lax.broadcasted_iota(jnp.int32, shape, 0)
    high = jnp.broadcast_to(high, shape)
    low = jnp.broadcast_to(low, shape)
    return jnp.where(row == 0, high, jnp.where(row == 1, low, 0.0)).astype(BF16)


def column(gain, l):
    return jnp.broadcast_to(gain[l : l + 1], (8, gain.shape[1])).T[:, :1]


def store_acts(out, at_row, value, gain_column):
    width = value.shape[0]
    out[at_row : at_row + width] = (value * gain_column).astype(BF16)
    squares = split_rows(jnp.sum(value * value, axis=0, keepdims=True))
    out[at_row + width : at_row + width + EXTRA] = squares


def fetched(refs, bufs, sems):
    copies = [pltpu.make_async_copy(r, b, sems.at[i]) for i, (r, b) in enumerate(zip(refs, bufs))]
    for c in copies:
        c.start()
    return copies


def store_quarter(turns, q, out):
    quarter = turns[0].shape[0] // SIDE
    start = pl.multiple_of(q * quarter, 16)
    for i, turn in enumerate(turns):
        out[i * quarter : (i + 1) * quarter] = turn[pl.ds(start, quarter)]


def turn_scratch(width, cols):
    return [
        pltpu.VMEM((width, cols), BF16),
        pltpu.VMEM((width, cols), BF16),
        pltpu.VMEM((cols, width), BF16),
        pltpu.VMEM((cols, width), BF16),
    ]


def first_pack(tokens, gain, gate_weight, up_weight, order):
    seqs, length, width = tokens.shape
    cols = gate_weight.shape[2]
    half = seqs // 2 * length
    quarter = cols // 2
    n = len(order)

    def kernel(tokens, gain, gate, up, *refs):
        outs, carried = refs[:n], refs[n]
        gate_buf, up_buf, *turns, token_buf, gain_buf, sems = refs[n + 1 :]
        core, first, _ = position()
        copies = fetched(
            (tokens, gain, gate.at[0], up.at[0]), (token_buf, gain_buf, gate_buf, up_buf), sems
        )
        copies[0].wait()
        copies[1].wait()
        gain_column = column(gain_buf, 0)
        for h in range(2):
            place = core ^ h
            mine = token_buf[pl.ds(place * (seqs // 2), seqs // 2)].reshape(half, width)
            value = mine.astype(F32).T
            if h == 0:
                carried[...] = value
            for out in outs:
                store_acts(out, quarter + h * (width + EXTRA), value, gain_column)
        for c, buf, turn in zip(copies[2:], (gate_buf, up_buf), turns):
            c.wait()
            turn[...] = buf[...].T
        for d, out in zip(order, outs):
            store_quarter(turns, first ^ d, out)

    outs = [array((quarter + 2 * (width + EXTRA), width), BF16)] * n
    outs.append(array((width, half), F32))
    return local(
        kernel,
        outs,
        *map(in_hbm, (tokens, gain, gate_weight, up_weight)),
        specs=[HBM] * 4,
        scratch=[
            *turn_scratch(width, cols),
            pltpu.VMEM(tokens.shape, BF16),
            pltpu.VMEM(gain.shape, F32),
            pltpu.SemaphoreType.DMA((4,)),
        ],
    )


def turn_in(gate_weight, up_weight, l):
    _, width, cols = gate_weight.shape
    quarter = cols // 2

    def kernel(gate, up, out, gate_buf, up_buf, *rest):
        *turns, sems = rest
        copies = fetched((gate.at[l], up.at[l]), (gate_buf, up_buf), sems)
        for c, buf, turn in zip(copies, (gate_buf, up_buf), turns):
            c.wait()
            turn[...] = buf[...].T
        for q in range(SIDE):
            store_quarter(turns, q, out.at[q * quarter : (q + 1) * quarter])

    return local(
        kernel,
        array((SIDE * quarter, width), BF16),
        *map(in_hbm, (gate_weight, up_weight)),
        specs=[HBM, HBM],
        scratch=[*turn_scratch(width, cols), pltpu.SemaphoreType.DMA((2,))],
    )


def mixed(mine, twins, order):
    rows, width = mine.shape
    quarter = rows // SIDE

    def kernel(mine, twins, *outs):
        _, first, _ = position()
        for d, out in zip(order, outs):
            start = pl.multiple_of((first ^ d) * quarter, 16)
            out[:quarter] = mine[pl.ds(start, quarter)]
            out[quarter:] = twins[pl.ds(start, quarter)]

    return local(kernel, [array((2 * quarter, width), BF16)] * len(order), mine, twins)


def turn_down(down_weight, l):
    _, cols, width = down_weight.shape
    quarter = cols // SIDE

    def kernel(weights, out, buf, sems):
        for c in fetched((weights.at[l],), (buf,), sems):
            c.wait()
        for q in range(SIDE):
            out[q, :, :quarter] = buf[q * quarter : (q + 1) * quarter].T

    return local(
        kernel,
        array((SIDE, width, pl.cdiv(quarter, 128) * 128), BF16),
        in_hbm(down_weight),
        specs=[HBM],
        scratch=[pltpu.VMEM((cols, width), BF16), pltpu.SemaphoreType.DMA((1,))],
    )


def pack_small(gate_taps, up_taps, gate_bias, up_bias):
    layers, cols = gate_bias.shape

    def kernel(gate_taps, up_taps, gate_bias, up_bias, out):
        for l in range(layers):
            rows = []
            for taps, bias in ((gate_taps, gate_bias), (up_taps, up_bias)):
                rows += [taps[t, l : l + 1] for t in range(KERNEL)] + [bias[l : l + 1]]
            out[l] = jnp.concatenate(rows, axis=0)

    turn = lambda taps: jnp.transpose(taps, (1, 0, 2))
    out = array((layers, 2 * (KERNEL + 1), cols), F32)
    return local(kernel, out, turn(gate_taps), turn(up_taps), gate_bias, up_bias)


def turn_small(mine, twins):
    layers, count, cols = mine.shape
    share = cols // (SIDE * SIDE)
    lanes = 128

    def kernel(mine, twins, out):
        _, first, second = position()
        shift = lax.rem(cols - (first * SIDE + second) * share, cols)
        for i, ref in enumerate((mine, twins)):
            for l in range(layers):
                out[i * layers + l] = pltpu.roll(ref[l], shift, 1)[:, :lanes].T

    return local(kernel, array((2 * layers, lanes, count), F32), mine, twins)


def added(carried, parts):
    a, b, c, d = (p[...].astype(F32) for p in parts)
    return resid_scale * carried[...] + ((a + b) + (c + d))


def next_block(carried, parts, gain, l):
    def kernel(carried, a, b, c, d, gain, out, acts):
        value = added(carried, (a, b, c, d))
        out[...] = value
        store_acts(acts, 0, value, column(gain, l))

    width, rows = carried.shape
    outs = [array((width, rows), F32), array((width + EXTRA, rows), BF16)]
    return local(kernel, outs, carried, *parts, gain)


def last_block(carried, parts, seqs, length):
    def kernel(carried, a, b, c, d, out):
        out[...] = added(carried, (a, b, c, d)).T.astype(BF16).reshape(out.shape)

    out = array((seqs, length, carried.shape[0]), BF16)
    return local(kernel, out, carried, *parts)


def joined(mine, other):
    seqs, length, width = mine.shape

    def kernel(mine, other, out):
        core, _, _ = position()
        out[pl.ds(core * seqs, seqs)] = mine[...]
        out[pl.ds((1 - core) * seqs, seqs)] = other[...]

    return local(kernel, array((2 * seqs, length, width), BF16), mine, other)


def products(unit, width, rows, operands, read, order):
    share = unit // SIDE
    stretches, count, step = rows

    def kernel(*refs):
        ins, outs, acc = refs[: len(operands)], refs[len(operands) : -1], refs[-1]
        _, _, second = position()
        for h in range(stretches):
            cut = slice(h * step, (h + 1) * step)
            total, squares = 0.0, 0.0
            for weights, acts, extra in read(ins, h):
                total = total + jnp.dot(weights, acts, preferred_element_type=F32)
                extra = extra.astype(F32)
                squares = squares + extra[0:1] + extra[1:2]
            acc[:, cut] = total
            squares = split_rows(squares)
            for out in outs:
                out[count // SIDE :, cut] = squares
        for d, out in zip(order, outs):
            start = pl.multiple_of((second ^ d) * share, 8)
            groups = [acc[pl.ds(start + g * unit, share)] for g in range(count // unit)]
            out[: count // SIDE] = jnp.concatenate(groups, axis=0).astype(BF16)

    tokens = stretches * step
    return local(
        kernel,
        [array((count // SIDE + EXTRA, tokens), BF16)] * len(order),
        *operands,
        flops=2 * count * SIDE * width * tokens,
        scratch=[pltpu.VMEM((count, tokens), F32)],
    )


def first_products(packs, unit, width, half, order):
    count = 2 * unit

    def read(refs, h):
        start = count + h * (width + EXTRA)
        for ref in refs:
            acts = ref[start : start + width]
            yield ref[:count], acts, ref[start + width : start + width + EXTRA]

    return products(unit, width, (2, count, half), packs, read, order)


def next_products(weights, acts, unit, width, half, order):
    n = len(weights)

    def read(refs, h):
        for w, a in zip(refs[:n], refs[n:]):
            yield w[...], a[:width], a[width:]

    return products(unit, width, (1, 4 * unit, half), [*weights, *acts], read, order)


def gated(parts, small, which, share, length):
    total, rows = parts[0].shape
    end = total - EXTRA

    def kernel(a, b, c, d, small, out):
        lane = lax.broadcasted_iota(jnp.int32, (share, length), 1)

        def conv(now, coef, k):
            one = jnp.where(lane >= 1, pltpu.roll(now, 1, 1), 0.0)
            two = jnp.where(lane >= 2, pltpu.roll(now, 2, 1), 0.0)
            early = coef[:, k + 3 : k + 4] + coef[:, k : k + 1] * two
            return early + coef[:, k + 1 : k + 2] * one + coef[:, k + 2 : k + 3] * now

        for s in range(rows // length):
            cut = slice(s * length, (s + 1) * length)
            a_, b_, c_, d_ = (p[:, cut].astype(F32) for p in (a, b, c, d))
            value = (a_ + b_) + (c_ + d_)
            row_squares = value[end : end + 1] + value[end + 1 : end + 2]
            inverse = lax.rsqrt(row_squares / D + eps)
            now = (value[:end] * inverse).astype(BF16).astype(F32)
            results = []
            for g, l in enumerate(which):
                coef = small[l, :share]
                gate = conv(now[2 * g * share : (2 * g + 1) * share], coef, 0)
                up = conv(now[(2 * g + 1) * share : (2 * g + 2) * share], coef, KERNEL + 1)
                results.append(gate / (1.0 + jnp.exp(-gate)) * up)
            out[:, cut] = jnp.concatenate(results, axis=0).astype(BF16)

    return local(kernel, array((end // 2, rows), BF16), *parts, small)


def collected(parts, share, ds):
    count, rows = parts[0].shape

    def kernel(*refs):
        out, buf = refs[SIDE], refs[SIDE + 1]
        _, _, second = position()
        for d, ref in zip(ds, refs):
            value = ref[...].astype(F32)
            for g in range(count // share):
                start = pl.multiple_of((g * SIDE + (second ^ d)) * share, 8)
                buf[pl.ds(start, share)] = value[g * share : (g + 1) * share]
        out[...] = buf[...].astype(BF16)

    out = array((SIDE * count, rows), BF16)
    scratch = [pltpu.VMEM((SIDE * count, rows), F32)]
    return local(kernel, out, *parts, scratch=scratch)


def mixed_down(sources, order):
    _, width, lanes = sources[0].shape
    m = len(sources)

    def kernel(*refs):
        _, first, _ = position()
        for d, out in zip(order, refs[m:]):
            for g in range(m):
                out[:, g * lanes : (g + 1) * lanes] = refs[g][first ^ d]

    outs = [array((width, m * lanes), BF16)] * len(order)
    return local(kernel, outs, *sources)


def spread(weights, groups, lanes, block):
    width = weights[0].shape[0]
    rows, tokens = block.shape
    n, unit = len(weights), rows // len(groups)

    def kernel(*refs):
        for w, out in zip(refs[:n], refs[n + 1 :]):
            total = 0.0
            for i, g in enumerate(groups):
                total = total + jnp.dot(
                    w[:, g * lanes : g * lanes + unit],
                    refs[n][i * unit : (i + 1) * unit],
                    preferred_element_type=F32,
                )
            out[...] = total.astype(BF16)

    flops = 2 * n * width * rows * tokens
    outs = [array((width, tokens), BF16)] * n
    return local(kernel, outs, *weights, block, flops=flops)


def summed(parts, dtypes):
    width, tokens = parts[0].shape
    step = tokens // len(dtypes)

    def kernel(a, b, c, d, *outs):
        for h, out in enumerate(outs):
            a_, b_, c_, d_ = (p[:, h * step : (h + 1) * step].astype(F32) for p in (a, b, c, d))
            out[...] = ((a_ + b_) + (c_ + d_)).astype(out.dtype)

    return local(kernel, [array((width, step), t) for t in dtypes], *parts)


def paired(mine, other):
    def kernel(mine, other, out):
        out[...] = (mine[...] + other[...].astype(F32)).astype(BF16)

    return local(kernel, array(mine.shape, BF16), mine, other)


def after(values, *earlier):
    return lax.optimization_barrier((values, *earlier))[0]


def per_device(
    tokens, norm_gain, gate_weight, up_weight, gate_taps, up_taps, gate_bias, up_bias, down_weight
):
    seqs, length, width = tokens.shape
    half = seqs // 2 * length
    unit = gate_weight.shape[2] // SIDE
    share = unit // SIDE
    every = tuple(range(SIDE))

    *packs, carried = first_pack(tokens, norm_gain, gate_weight, up_weight, every)
    mine = turn_in(gate_weight, up_weight, 1)
    turned = mixed(mine, to_twin(mine), every)
    downs = []
    for l in range(LAYERS):
        downs.append(turn_down(down_weight, l))
    lanes = downs[0].shape[2]
    downs = [mixed_down(downs[:1], every), mixed_down([downs[1], to_twin(downs[1])], every)]
    small = pack_small(gate_taps, up_taps, gate_bias, up_bias)
    small = turn_small(small, to_twin(small))
    got = moved(first_move, packs)
    got = after(got, downs, turned, small)
    got = [packs[0], *(got[d] for d in every[1:])]
    late = moved(first_move, downs[0])
    late = [downs[0][0], late[1], late[2], late[3]]
    parts = first_products(got, unit, width, half, every)
    for l in range(LAYERS):
        got = moved(second_move, parts)
        which = (0,) if l == 0 else (1, LAYERS + 1)
        hidden = gated([parts[0], got[1], got[2], got[3]], small, which, share, length)
        got = moved(second_move, [hidden] * SIDE)
        block = collected([hidden, got[1], got[2], got[3]], share, every)
        branch = spread(late, range(l + 1), lanes, block)
        got = moved(first_move, branch)
        got = [branch[0], got[1], got[2], got[3]]
        if l == 0:
            weights = moved(first_move, after(turned, block))
            weights = [turned[0], weights[1], weights[2], weights[3]]
            mine, twins = summed(got, [F32, BF16])
            branch = paired(mine, to_twin(twins))
        else:
            (branch,) = summed(got, [BF16])
        got = moved(x_move, [branch] * SIDE)
        got = [branch, got[1], got[2], got[3]]
        if l == 0:
            carried, acts = next_block(carried, got, norm_gain, l + 1)
            got = moved(first_move, [acts] * SIDE)
            got = [acts, got[1], got[2], got[3]]
            late = moved(first_move, after(downs[1], acts))
            late = [downs[1][0], late[1], late[2], late[3]]
            parts = next_products(weights, got, unit, width, half, every)
    mine = last_block(carried, got, seqs // 2, length)
    return joined(mine, to_twin(mine))


def solution(mesh):
    in_specs = (
        P(None, None, "ra"),
        P(None, "ra"),
        P(None, "ra", "cb"),
        P(None, "ra", "cb"),
        P(None, None, "cb"),
        P(None, None, "cb"),
        P(None, "cb"),
        P(None, "cb"),
        P(None, "cb", "ra"),
    )
    out_specs = P(None, None, "ra")

    return jax.shard_map(
        per_device, mesh=mesh, in_specs=in_specs, out_specs=out_specs, check_vma=False
    )
```

profile of v0, /device:TPU:1, one launch (start us, length us, event | category | flops | bytes accessed | tf_op | source)
XLA Modules:
  0.0 154.7 jit_solution(4389718587207829277)
XLA Ops:
  0.0 1.6 %shard_map.96.mine = bf16[2816,256]{1,0:T(8,128)(2,1)S(1)} custom-call(bf16[2,256,1408]{2,1,0:T(8,128)(2,1)} %gate.3, bf16[2,256,1408]{2,1,0:T(8,128)(2,1)} %up.3), custom_call_target="tpu_custom_call" | custom-call | flops 1000000000 | bytes 2883584 | tf_op jit(solution)/shard_map/pallas_call | solution.py:71
  1.7 1.5 collective-permute-start.7
  3.2 1.4 shard_map.94.refs_0_
  4.7 0.5 collective-permute-start.8
  5.3 1.9 %shard_map.91 = (bf16[1248,256]{1,0:T(8,128)(2,1)S(1)}, bf16[1248,256]{1,0:T(8,128)(2,1)S(1)}, bf16[1248,256]{1,0:T(8,128)(2,1)S(1)}, bf16[1248,256]{1,0:T(8,128)(2,1)S(1)}, f32[256,256]{1,0:T(8,128)S(1)}) custom-call(bf16[4,128,256]{2,1,0:T(8,128)(2,1)} %tokens.1, f32[2,256]{1,0:T(2,128)} %gain.3, bf16[2,256,1408]{2,1,0:T(8,128)(2,1)} %gate.3, ...), custom_call_target="tpu_custom_call" | custom-call | flops 1000000000 | bytes 3147776 | tf_op jit(solution)/shard_map/pallas_call | solution.py:71
  7.2 1.5 collective-permute-start.3
  8.7 2.6 %collective-permute-start.4 = (bf16[1248,256]{1,0:T(8,128)(2,1)S(1)}, bf16[1248,256]{1,0:T(8,128)(2,1)S(1)}, u32[]{:S(2)}, u32[]{:S(2)}) collective-permute-start(bf16[1248,256]{1,0:T(8,128)(2,1)S(1)} %get-tuple-element.58), channel_id=1, source_target_pairs={{0,64},{1,17},{2,66},{3,19},{4,68},{5,21},{6,70},{7,23},{8,72},{9,... | collective-permute-start | bytes 1916936 | tf_op jit(solution)/shard_map/ppermute | solution.py:54
  11.3 1.4 shard_map.92.refs_0_
  13.5 3.4 %collective-permute-done.3.refs_1_ = bf16[1248,256]{1,0:T(8,128)(2,1)S(1)} collective-permute-done((bf16[1248,256]{1,0:T(8,128)(2,1)S(1)}, bf16[1248,256]{1,0:T(8,128)(2,1)S(1)}, u32[]{:S(2)}, u32[]{:S(2)}) %collective-permute-start.3) | collective-permute-done | bytes 639008 | tf_op jit(solution)/shard_map/ppermute | solution.py:54
  16.8 9.5 %collective-permute-done.4.refs_2_ = bf16[1248,256]{1,0:T(8,128)(2,1)S(1)} collective-permute-done((bf16[1248,256]{1,0:T(8,128)(2,1)S(1)}, bf16[1248,256]{1,0:T(8,128)(2,1)S(1)}, u32[]{:S(2)}, u32[]{:S(2)}) %collective-permute-start.4) | collective-permute-done | bytes 639008 | tf_op jit(solution)/shard_map/ppermute | solution.py:54
  26.3 2.6 %collective-permute-done.5.refs_3_ = bf16[1248,256]{1,0:T(8,128)(2,1)S(1)} collective-permute-done((bf16[1248,256]{1,0:T(8,128)(2,1)S(1)}, bf16[1248,256]{1,0:T(8,128)(2,1)S(1)}, u32[]{:S(2)}, u32[]{:S(2)}) %collective-permute-start.5) | collective-permute-done | bytes 639008 | tf_op jit(solution)/shard_map/ppermute | solution.py:54
  28.9 1.0 shard_map.100
  29.9 3.4 %collective-permute-start.10 = (bf16[192,512]{1,0:T(8,128)(2,1)S(1)}, bf16[192,512]{1,0:T(8,128)(2,1)S(1)}, u32[]{:S(2)}, u32[]{:S(2)}) collective-permute-start(bf16[192,512]{1,0:T(8,128)(2,1)S(1)} %get-tuple-element.73), channel_id=1, source_target_pairs={{0,16},{1,65},{2,18},{3,67},{4,20},{5,69},{6,22},{7,71},{8,24},{9,... | collective-permute-start | bytes 589832 | tf_op jit(solution)/shard_map/ppermute | solution.py:54
  34.1 2.3 %collective-permute-done.10.c = bf16[192,512]{1,0:T(8,128)(2,1)S(1)} collective-permute-done((bf16[192,512]{1,0:T(8,128)(2,1)S(1)}, bf16[192,512]{1,0:T(8,128)(2,1)S(1)}, u32[]{:S(2)}, u32[]{:S(2)}) %collective-permute-start.10) | collective-permute-done | bytes 196640 | tf_op jit(solution)/shard_map/ppermute | solution.py:54
  36.4 2.9 %collective-permute-done.11.d = bf16[192,512]{1,0:T(8,128)(2,1)S(1)} collective-permute-done((bf16[192,512]{1,0:T(8,128)(2,1)S(1)}, bf16[192,512]{1,0:T(8,128)(2,1)S(1)}, u32[]{:S(2)}, u32[]{:S(2)}) %collective-permute-start.11) | collective-permute-done | bytes 196640 | tf_op jit(solution)/shard_map/ppermute | solution.py:54
  39.3 0.6 shard_map.101.refs_0_
  39.9 1.1 collective-permute-start.12
  41.0 1.2 collective-permute-start.1
  42.2 2.7 %collective-permute-start.2 = (bf16[256,384]{1,0:T(8,128)(2,1)S(1)}, bf16[256,384]{1,0:T(8,128)(2,1)S(1)}, u32[]{:S(2)}, u32[]{:S(2)}) collective-permute-start(bf16[256,384]{1,0:T(8,128)(2,1)S(1)} %get-tuple-element.55), channel_id=1, source_target_pairs={{0,96},{1,25},{2,98},{3,27},{4,100},{5,29},{6,102},{7,31},{8,104},... | collective-permute-start | bytes 589832 | tf_op jit(solution)/shard_map/ppermute | solution.py:54
  44.9 2.8 %collective-permute-start.13 = (bf16[88,512]{1,0:T(8,128)(2,1)S(1)}, bf16[88,512]{1,0:T(8,128)(2,1)S(1)}, u32[]{:S(2)}, u32[]{:S(2)}) collective-permute-start(bf16[88,512]{1,0:T(8,128)(2,1)S(1)} %shard_map.101.refs_0_), channel_id=1, source_target_pairs={{0,16},{1,65},{2,18},{3,67},{4,20},{5,69},{6,22},{7,71},{8,24},{9,... | collective-permute-start | bytes 270344 | tf_op jit(solution)/shard_map/ppermute | solution.py:54
  47.7 3.3 %collective-permute-done.13.refs_2_ = bf16[88,512]{1,0:T(8,128)(2,1)S(1)} collective-permute-done((bf16[88,512]{1,0:T(8,128)(2,1)S(1)}, bf16[88,512]{1,0:T(8,128)(2,1)S(1)}, u32[]{:S(2)}, u32[]{:S(2)}) %collective-permute-start.13) | collective-permute-done | bytes 90144 | tf_op jit(solution)/shard_map/ppermute | solution.py:54
  51.0 3.0 %collective-permute-done.14.refs_3_ = bf16[88,512]{1,0:T(8,128)(2,1)S(1)} collective-permute-done((bf16[88,512]{1,0:T(8,128)(2,1)S(1)}, bf16[88,512]{1,0:T(8,128)(2,1)S(1)}, u32[]{:S(2)}, u32[]{:S(2)}) %collective-permute-start.14) | collective-permute-done | bytes 90144 | tf_op jit(solution)/shard_map/ppermute | solution.py:54
  54.2 0.7 shard_map.103
  55.0 2.2 %collective-permute-start.16 = (bf16[256,512]{1,0:T(8,128)(2,1)S(1)}, bf16[256,512]{1,0:T(8,128)(2,1)S(1)}, u32[]{:S(2)}, u32[]{:S(2)}) collective-permute-start(bf16[256,512]{1,0:T(8,128)(2,1)S(1)} %get-tuple-element.77), channel_id=1, source_target_pairs={{0,64},{1,17},{2,66},{3,19},{4,68},{5,21},{6,70},{7,23},{8,72},{9,... | collective-permute-start | bytes 786440 | tf_op jit(solution)/shard_map/ppermute | solution.py:54
  57.2 1.6 %collective-permute-start.17 = (bf16[256,512]{1,0:T(8,128)(2,1)S(1)}, bf16[256,512]{1,0:T(8,128)(2,1)S(1)}, u32[]{:S(2)}, u32[]{:S(2)}) collective-permute-start(bf16[256,512]{1,0:T(8,128)(2,1)S(1)} %get-tuple-element.78), channel_id=1, source_target_pairs={{0,96},{1,25},{2,98},{3,27},{4,100},{5,29},{6,102},{7,31},{8,104},... | collective-permute-start | bytes 786440 | tf_op jit(solution)/shard_map/ppermute | solution.py:54
  58.8 1.4 collective-permute-done.15.b
  60.2 3.7 %collective-permute-done.16.c = bf16[256,512]{1,0:T(8,128)(2,1)S(1)} collective-permute-done((bf16[256,512]{1,0:T(8,128)(2,1)S(1)}, bf16[256,512]{1,0:T(8,128)(2,1)S(1)}, u32[]{:S(2)}, u32[]{:S(2)}) %collective-permute-start.16) | collective-permute-done | bytes 262176 | tf_op jit(solution)/shard_map/ppermute | solution.py:54
  63.8 2.9 %collective-permute-done.17.d = bf16[256,512]{1,0:T(8,128)(2,1)S(1)} collective-permute-done((bf16[256,512]{1,0:T(8,128)(2,1)S(1)}, bf16[256,512]{1,0:T(8,128)(2,1)S(1)}, u32[]{:S(2)}, u32[]{:S(2)}) %collective-permute-start.17) | collective-permute-done | bytes 262176 | tf_op jit(solution)/shard_map/ppermute | solution.py:54
  66.8 3.6 %collective-permute-start.18 = (bf16[256,256]{1,0:T(8,128)(2,1)S(1)}, bf16[256,256]{1,0:T(8,128)(2,1)S(1)}, u32[]{:S(2)}, u32[]{:S(2)}) collective-permute-start(bf16[256,256]{1,0:T(8,128)(2,1)S(1)} %get-tuple-element.80), channel_id=1, source_target_pairs={{0,1},{1,0},{2,3},{3,2},{4,5},{5,4},{6,7},{7,6},{8,9},{9,8},{10,11... | collective-permute-start | bytes 393224 | tf_op jit(solution)/shard_map/ppermute | solution.py:36
  70.4 2.0 %collective-permute-start.26 = (bf16[1408,256]{1,0:T(8,128)(2,1)S(1)}, bf16[1408,256]{1,0:T(8,128)(2,1)S(1)}, u32[]{:S(2)}, u32[]{:S(2)}) collective-permute-start(bf16[1408,256]{1,0:T(8,128)(2,1)S(1)} %get-tuple-element.87), channel_id=1, source_target_pairs={{0,64},{1,17},{2,66},{3,19},{4,68},{5,21},{6,70},{7,23},{8,72},{9,... | collective-permute-start | bytes 2162696 | tf_op jit(solution)/shard_map/ppermute | solution.py:54
  72.4 1.8 %collective-permute-start.27 = (bf16[1408,256]{1,0:T(8,128)(2,1)S(1)}, bf16[1408,256]{1,0:T(8,128)(2,1)S(1)}, u32[]{:S(2)}, u32[]{:S(2)}) collective-permute-start(bf16[1408,256]{1,0:T(8,128)(2,1)S(1)} %get-tuple-element.88), channel_id=1, source_target_pairs={{0,96},{1,25},{2,98},{3,27},{4,100},{5,29},{6,102},{7,31},{8,104},... | collective-permute-start | bytes 2162696 | tf_op jit(solution)/shard_map/ppermute | solution.py:54
  74.3 1.3 collective-permute-start.19
  75.6 2.5 %collective-permute-start.20 = (bf16[256,256]{1,0:T(8,128)(2,1)S(1)}, bf16[256,256]{1,0:T(8,128)(2,1)S(1)}, u32[]{:S(2)}, u32[]{:S(2)}) collective-permute-start(bf16[256,256]{1,0:T(8,128)(2,1)S(1)} %shard_map.105.a), channel_id=1, source_target_pairs={{0,4},{1,5},{2,6},{3,7},{4,0},{5,1},{6,2},{7,3},{8,12},{9,13},{10,... | collective-permute-start | bytes 393224 | tf_op jit(solution)/shard_map/ppermute | solution.py:54
  78.1 0.5 collective-permute-done.19.b
  78.5 2.5 %collective-permute-start.21 = (bf16[256,256]{1,0:T(8,128)(2,1)S(1)}, bf16[256,256]{1,0:T(8,128)(2,1)S(1)}, u32[]{:S(2)}, u32[]{:S(2)}) collective-permute-start(bf16[256,256]{1,0:T(8,128)(2,1)S(1)} %shard_map.105.a), channel_id=1, source_target_pairs={{0,6},{1,7},{2,4},{3,5},{4,2},{5,3},{6,0},{7,1},{8,14},{9,15},{10,... | collective-permute-start | bytes 393224 | tf_op jit(solution)/shard_map/ppermute | solution.py:54
  81.0 2.5 %collective-permute-done.20.c = bf16[256,256]{1,0:T(8,128)(2,1)S(1)} collective-permute-done((bf16[256,256]{1,0:T(8,128)(2,1)S(1)}, bf16[256,256]{1,0:T(8,128)(2,1)S(1)}, u32[]{:S(2)}, u32[]{:S(2)}) %collective-permute-start.20) | collective-permute-done | bytes 131104 | tf_op jit(solution)/shard_map/ppermute | solution.py:54
  83.5 2.5 %collective-permute-done.21.d = bf16[256,256]{1,0:T(8,128)(2,1)S(1)} collective-permute-done((bf16[256,256]{1,0:T(8,128)(2,1)S(1)}, bf16[256,256]{1,0:T(8,128)(2,1)S(1)}, u32[]{:S(2)}, u32[]{:S(2)}) %collective-permute-start.21) | collective-permute-done | bytes 131104 | tf_op jit(solution)/shard_map/ppermute | solution.py:54
  86.3 2.0 %collective-permute-start.29 = (bf16[272,256]{1,0:T(8,128)(2,1)S(1)}, bf16[272,256]{1,0:T(8,128)(2,1)S(1)}, u32[]{:S(2)}, u32[]{:S(2)}) collective-permute-start(bf16[272,256]{1,0:T(8,128)(2,1)S(1)} %get-tuple-element.82.refs_4_), channel_id=1, source_target_pairs={{0,64},{1,17},{2,66},{3,19},{4,68},{5,21},{6,70},{7,23},{8,72},{9,... | collective-permute-start | bytes 417800 | tf_op jit(solution)/shard_map/ppermute | solution.py:54
  88.3 2.2 %collective-permute-done.28.refs_5_ = bf16[272,256]{1,0:T(8,128)(2,1)S(1)} collective-permute-done((bf16[272,256]{1,0:T(8,128)(2,1)S(1)}, bf16[272,256]{1,0:T(8,128)(2,1)S(1)}, u32[]{:S(2)}, u32[]{:S(2)}) %collective-permute-start.28) | collective-permute-done | bytes 139296 | tf_op jit(solution)/shard_map/ppermute | solution.py:54
  90.5 0.8 collective-permute-start.30
  91.4 1.0 collective-permute-done.29.refs_6_
  92.4 3.6 %collective-permute-done.30.refs_7_ = bf16[272,256]{1,0:T(8,128)(2,1)S(1)} collective-permute-done((bf16[272,256]{1,0:T(8,128)(2,1)S(1)}, bf16[272,256]{1,0:T(8,128)(2,1)S(1)}, u32[]{:S(2)}, u32[]{:S(2)}) %collective-permute-start.30) | collective-permute-done | bytes 139296 | tf_op jit(solution)/shard_map/ppermute | solution.py:54
  96.0 1.0 shard_map.107
  97.1 3.4 %collective-permute-start.32 = (bf16[368,256]{1,0:T(8,128)(2,1)S(1)}, bf16[368,256]{1,0:T(8,128)(2,1)S(1)}, u32[]{:S(2)}, u32[]{:S(2)}) collective-permute-start(bf16[368,256]{1,0:T(8,128)(2,1)S(1)} %get-tuple-element.91), channel_id=1, source_target_pairs={{0,16},{1,65},{2,18},{3,67},{4,20},{5,69},{6,22},{7,71},{8,24},{9,... | collective-permute-start | bytes 565256 | tf_op jit(solution)/shard_map/ppermute | solution.py:54
  100.9 2.0 %collective-permute-start.23 = (bf16[256,768]{1,0:T(8,128)(2,1)S(1)}, bf16[256,768]{1,0:T(8,128)(2,1)S(1)}, u32[]{:S(2)}, u32[]{:S(2)}) collective-permute-start(bf16[256,768]{1,0:T(8,128)(2,1)S(1)} %get-tuple-element.84), channel_id=1, source_target_pairs={{0,64},{1,17},{2,66},{3,19},{4,68},{5,21},{6,70},{7,23},{8,72},{9,... | collective-permute-start | bytes 1179656 | tf_op jit(solution)/shard_map/ppermute | solution.py:54
  103.0 1.8 %collective-permute-start.24 = (bf16[256,768]{1,0:T(8,128)(2,1)S(1)}, bf16[256,768]{1,0:T(8,128)(2,1)S(1)}, u32[]{:S(2)}, u32[]{:S(2)}) collective-permute-start(bf16[256,768]{1,0:T(8,128)(2,1)S(1)} %get-tuple-element.85), channel_id=1, source_target_pairs={{0,96},{1,25},{2,98},{3,27},{4,100},{5,29},{6,102},{7,31},{8,104},... | collective-permute-start | bytes 1179656 | tf_op jit(solution)/shard_map/ppermute | solution.py:54
  104.8 0.8 collective-permute-done.32.c
  105.6 2.2 %collective-permute-done.33.d = bf16[368,256]{1,0:T(8,128)(2,1)S(1)} collective-permute-done((bf16[368,256]{1,0:T(8,128)(2,1)S(1)}, bf16[368,256]{1,0:T(8,128)(2,1)S(1)}, u32[]{:S(2)}, u32[]{:S(2)}) %collective-permute-start.33) | collective-permute-done | bytes 188448 | tf_op jit(solution)/shard_map/ppermute | solution.py:54
  107.8 0.6 shard_map.108.refs_0_
  108.5 1.3 collective-permute-start.35
  109.8 3.3 %collective-permute-done.34.refs_1_ = bf16[176,256]{1,0:T(8,128)(2,1)S(1)} collective-permute-done((bf16[176,256]{1,0:T(8,128)(2,1)S(1)}, bf16[176,256]{1,0:T(8,128)(2,1)S(1)}, u32[]{:S(2)}, u32[]{:S(2)}) %collective-permute-start.34) | collective-permute-done | bytes 90144 | tf_op jit(solution)/shard_map/ppermute | solution.py:54
  113.3 1.4 collective-permute-done.35.refs_2_
  114.6 8.3 %collective-permute-done.36.refs_3_ = bf16[176,256]{1,0:T(8,128)(2,1)S(1)} collective-permute-done((bf16[176,256]{1,0:T(8,128)(2,1)S(1)}, bf16[176,256]{1,0:T(8,128)(2,1)S(1)}, u32[]{:S(2)}, u32[]{:S(2)}) %collective-permute-start.36) | collective-permute-done | bytes 90144 | tf_op jit(solution)/shard_map/ppermute | solution.py:54
  123.0 0.7 shard_map.110
  123.8 1.9 %collective-permute-start.38 = (bf16[256,256]{1,0:T(8,128)(2,1)S(1)}, bf16[256,256]{1,0:T(8,128)(2,1)S(1)}, u32[]{:S(2)}, u32[]{:S(2)}) collective-permute-start(bf16[256,256]{1,0:T(8,128)(2,1)S(1)} %get-tuple-element.95), channel_id=1, source_target_pairs={{0,64},{1,17},{2,66},{3,19},{4,68},{5,21},{6,70},{7,23},{8,72},{9,... | collective-permute-start | bytes 393224 | tf_op jit(solution)/shard_map/ppermute | solution.py:54
  125.7 2.0 %collective-permute-start.39 = (bf16[256,256]{1,0:T(8,128)(2,1)S(1)}, bf16[256,256]{1,0:T(8,128)(2,1)S(1)}, u32[]{:S(2)}, u32[]{:S(2)}) collective-permute-start(bf16[256,256]{1,0:T(8,128)(2,1)S(1)} %get-tuple-element.96), channel_id=1, source_target_pairs={{0,96},{1,25},{2,98},{3,27},{4,100},{5,29},{6,102},{7,31},{8,104},... | collective-permute-start | bytes 393224 | tf_op jit(solution)/shard_map/ppermute | solution.py:54
  127.9 1.6 %collective-permute-done.38.c = bf16[256,256]{1,0:T(8,128)(2,1)S(1)} collective-permute-done((bf16[256,256]{1,0:T(8,128)(2,1)S(1)}, bf16[256,256]{1,0:T(8,128)(2,1)S(1)}, u32[]{:S(2)}, u32[]{:S(2)}) %collective-permute-start.38) | collective-permute-done | bytes 131104 | tf_op jit(solution)/shard_map/ppermute | solution.py:54
  129.6 1.6 %collective-permute-done.39.d = bf16[256,256]{1,0:T(8,128)(2,1)S(1)} collective-permute-done((bf16[256,256]{1,0:T(8,128)(2,1)S(1)}, bf16[256,256]{1,0:T(8,128)(2,1)S(1)}, u32[]{:S(2)}, u32[]{:S(2)}) %collective-permute-start.39) | collective-permute-done | bytes 131104 | tf_op jit(solution)/shard_map/ppermute | solution.py:54
  131.3 3.9 %collective-permute-start.41 = (bf16[256,256]{1,0:T(8,128)(2,1)S(1)}, bf16[256,256]{1,0:T(8,128)(2,1)S(1)}, u32[]{:S(2)}, u32[]{:S(2)}) collective-permute-start(bf16[256,256]{1,0:T(8,128)(2,1)S(1)} %shard_map.111.a), channel_id=1, source_target_pairs={{0,4},{1,5},{2,6},{3,7},{4,0},{5,1},{6,2},{7,3},{8,12},{9,13},{10,... | collective-permute-start | bytes 393224 | tf_op jit(solution)/shard_map/ppermute | solution.py:54
  135.4 3.9 %collective-permute-done.41.c = bf16[256,256]{1,0:T(8,128)(2,1)S(1)} collective-permute-done((bf16[256,256]{1,0:T(8,128)(2,1)S(1)}, bf16[256,256]{1,0:T(8,128)(2,1)S(1)}, u32[]{:S(2)}, u32[]{:S(2)}) %collective-permute-start.41) | collective-permute-done | bytes 131104 | tf_op jit(solution)/shard_map/ppermute | solution.py:54
  139.3 1.4 collective-permute-done.42.d
  140.8 12.1 %collective-permute-start.43 = (bf16[2,128,256]{2,1,0:T(8,128)(2,1)S(1)}, bf16[2,128,256]{2,1,0:T(8,128)(2,1)S(1)}, u32[]{:S(2)}, u32[]{:S(2)}) collective-permute-start(bf16[2,128,256]{2,1,0:T(8,128)(2,1)S(1)} %shard_map.112.mine), channel_id=1, source_target_pairs={{0,1},{1,0},{2,3},{3,2},{4,5},{5,4},{6,7},{7,6},{8,9},{9,8},{10,11... | collective-permute-start | bytes 393224 | tf_op jit(solution)/shard_map/ppermute | solution.py:36
  152.9 1.0 collective-permute-done.43.other
  153.9 0.7 shard_map.113
  (57 shorter events, 4.0 us)
Async XLA Ops:
  1.7 3.0 %copy-start = (f32[2,3,1408]{2,0,1:T(2,128)S(1)}, f32[2,3,1408]{2,0,1:T(2,128)}, u32[]{:S(2)}) copy-start(f32[2,3,1408]{2,0,1:T(2,128)} %param.13) | copy-start | bytes 101380
  1.7 3.0 %copy-start.1 = (f32[2,3,1408]{2,0,1:T(2,128)S(1)}, f32[2,3,1408]{2,0,1:T(2,128)}, u32[]{:S(2)}) copy-start(f32[2,3,1408]{2,0,1:T(2,128)} %param.14) | copy-start | bytes 101380
  1.7 3.0 %copy-start.2 = (f32[2,1408]{1,0:T(2,128)S(1)}, f32[2,1408]{1,0:T(2,128)}, u32[]{:S(2)}) copy-start(f32[2,1408]{1,0:T(2,128)} %gate_bias.1) | copy-start | bytes 33796
  1.7 3.0 %copy-start.3 = (f32[2,1408]{1,0:T(2,128)S(1)}, f32[2,1408]{1,0:T(2,128)}, u32[]{:S(2)}) copy-start(f32[2,1408]{1,0:T(2,128)} %up_bias.1) | copy-start | bytes 33796
  1.7 11.5 %collective-permute-start.7 = (bf16[2816,256]{1,0:T(8,128)(2,1)S(1)}, bf16[2816,256]{1,0:T(8,128)(2,1)S(1)}, u32[]{:S(2)}, u32[]{:S(2)}) collective-permute-start(bf16[2816,256]{1,0:T(8,128)(2,1)S(1)} %shard_map.96.mine), channel_id=1, source_target_pairs={{0,1},{1,0},{2,3},{3,2},{4,5},{5,4},{6,7},{7,6},{8,9},{9,8},{10,11... | collective-permute-start | bytes 4325384 | tf_op jit(solution)/shard_map/ppermute | solution.py:36
  4.6 8.5 %collective-permute-start.6 = (bf16[4,256,384]{2,1,0:T(8,128)(2,1)S(1)}, bf16[4,256,384]{2,1,0:T(8,128)(2,1)S(1)}, u32[]{:S(2)}, u32[]{:S(2)}) collective-permute-start(bf16[4,256,384]{2,1,0:T(8,128)(2,1)S(1)} %shard_map.94.refs_0_), channel_id=1, source_target_pairs={{0,1},{1,0},{2,3},{3,2},{4,5},{5,4},{6,7},{7,6},{8,9},{9,8},{10,11... | collective-permute-start | bytes 2359304 | tf_op jit(solution)/shard_map/ppermute | solution.py:36
  4.7 6.6 %collective-permute-start.8 = (f32[2,8,1408]{2,1,0:T(8,128)S(1)}, f32[2,8,1408]{2,1,0:T(8,128)S(1)}, u32[]{:S(2)}, u32[]{:S(2)}) collective-permute-start(f32[2,8,1408]{2,1,0:T(8,128)S(1)} %shard_map.98.mine), channel_id=1, source_target_pairs={{0,1},{1,0},{2,3},{3,2},{4,5},{5,4},{6,7},{7,6},{8,9},{9,8},{10,11... | collective-permute-start | bytes 270344 | tf_op jit(solution)/shard_map/ppermute | solution.py:36
  7.2 9.6 %collective-permute-start.3 = (bf16[1248,256]{1,0:T(8,128)(2,1)S(1)}, bf16[1248,256]{1,0:T(8,128)(2,1)S(1)}, u32[]{:S(2)}, u32[]{:S(2)}) collective-permute-start(bf16[1248,256]{1,0:T(8,128)(2,1)S(1)} %get-tuple-element.57), channel_id=1, source_target_pairs={{0,32},{1,9},{2,34},{3,11},{4,36},{5,13},{6,38},{7,15},{8,40},{9,1... | collective-permute-start | bytes 1916936 | tf_op jit(solution)/shard_map/ppermute | solution.py:54
  8.7 17.6 %collective-permute-start.4 = (bf16[1248,256]{1,0:T(8,128)(2,1)S(1)}, bf16[1248,256]{1,0:T(8,128)(2,1)S(1)}, u32[]{:S(2)}, u32[]{:S(2)}) collective-permute-start(bf16[1248,256]{1,0:T(8,128)(2,1)S(1)} %get-tuple-element.58), channel_id=1, source_target_pairs={{0,64},{1,17},{2,66},{3,19},{4,68},{5,21},{6,70},{7,23},{8,72},{9,... | collective-permute-start | bytes 1916936 | tf_op jit(solution)/shard_map/ppermute | solution.py:54
  11.3 17.6 %collective-permute-start.5 = (bf16[1248,256]{1,0:T(8,128)(2,1)S(1)}, bf16[1248,256]{1,0:T(8,128)(2,1)S(1)}, u32[]{:S(2)}, u32[]{:S(2)}) collective-permute-start(bf16[1248,256]{1,0:T(8,128)(2,1)S(1)} %get-tuple-element.59), channel_id=1, source_target_pairs={{0,96},{1,25},{2,98},{3,27},{4,100},{5,29},{6,102},{7,31},{8,104},... | collective-permute-start | bytes 1916936 | tf_op jit(solution)/shard_map/ppermute | solution.py:54
  29.9 6.4 %collective-permute-start.10 = (bf16[192,512]{1,0:T(8,128)(2,1)S(1)}, bf16[192,512]{1,0:T(8,128)(2,1)S(1)}, u32[]{:S(2)}, u32[]{:S(2)}) collective-permute-start(bf16[192,512]{1,0:T(8,128)(2,1)S(1)} %get-tuple-element.73), channel_id=1, source_target_pairs={{0,16},{1,65},{2,18},{3,67},{4,20},{5,69},{6,22},{7,71},{8,24},{9,... | collective-permute-start | bytes 589832 | tf_op jit(solution)/shard_map/ppermute | solution.py:54
  33.3 6.0 %collective-permute-start.11 = (bf16[192,512]{1,0:T(8,128)(2,1)S(1)}, bf16[192,512]{1,0:T(8,128)(2,1)S(1)}, u32[]{:S(2)}, u32[]{:S(2)}) collective-permute-start(bf16[192,512]{1,0:T(8,128)(2,1)S(1)} %get-tuple-element.74), channel_id=1, source_target_pairs={{0,24},{1,97},{2,26},{3,99},{4,28},{5,101},{6,30},{7,103},{8,16},{... | collective-permute-start | bytes 589832 | tf_op jit(solution)/shard_map/ppermute | solution.py:54
  33.8 5.5 %collective-permute-start.9 = (bf16[192,512]{1,0:T(8,128)(2,1)S(1)}, bf16[192,512]{1,0:T(8,128)(2,1)S(1)}, u32[]{:S(2)}, u32[]{:S(2)}) collective-permute-start(bf16[192,512]{1,0:T(8,128)(2,1)S(1)} %get-tuple-element.72), channel_id=1, source_target_pairs={{0,8},{1,33},{2,10},{3,35},{4,12},{5,37},{6,14},{7,39},{8,0},{9,41... | collective-permute-start | bytes 589832 | tf_op jit(solution)/shard_map/ppermute | solution.py:54
  39.9 7.7 %collective-permute-start.12 = (bf16[88,512]{1,0:T(8,128)(2,1)S(1)}, bf16[88,512]{1,0:T(8,128)(2,1)S(1)}, u32[]{:S(2)}, u32[]{:S(2)}) collective-permute-start(bf16[88,512]{1,0:T(8,128)(2,1)S(1)} %shard_map.101.refs_0_), channel_id=1, source_target_pairs={{0,8},{1,33},{2,10},{3,35},{4,12},{5,37},{6,14},{7,39},{8,0},{9,41... | collective-permute-start | bytes 270344 | tf_op jit(solution)/shard_map/ppermute | solution.py:54
  41.0 13.1 %collective-permute-start = (bf16[256,384]{1,0:T(8,128)(2,1)S(1)}, bf16[256,384]{1,0:T(8,128)(2,1)S(1)}, u32[]{:S(2)}, u32[]{:S(2)}) collective-permute-start(bf16[256,384]{1,0:T(8,128)(2,1)S(1)} %get-tuple-element.53), channel_id=1, source_target_pairs={{0,32},{1,9},{2,34},{3,11},{4,36},{5,13},{6,38},{7,15},{8,40},{9,1... | collective-permute-start | bytes 589832 | tf_op jit(solution)/shard_map/ppermute | solution.py:54
  41.0 13.1 %collective-permute-start.1 = (bf16[256,384]{1,0:T(8,128)(2,1)S(1)}, bf16[256,384]{1,0:T(8,128)(2,1)S(1)}, u32[]{:S(2)}, u32[]{:S(2)}) collective-permute-start(bf16[256,384]{1,0:T(8,128)(2,1)S(1)} %get-tuple-element.54), channel_id=1, source_target_pairs={{0,64},{1,17},{2,66},{3,19},{4,68},{5,21},{6,70},{7,23},{8,72},{9,... | collective-permute-start | bytes 589832 | tf_op jit(solution)/shard_map/ppermute | solution.py:54
  42.2 12.0 %collective-permute-start.2 = (bf16[256,384]{1,0:T(8,128)(2,1)S(1)}, bf16[256,384]{1,0:T(8,128)(2,1)S(1)}, u32[]{:S(2)}, u32[]{:S(2)}) collective-permute-start(bf16[256,384]{1,0:T(8,128)(2,1)S(1)} %get-tuple-element.55), channel_id=1, source_target_pairs={{0,96},{1,25},{2,98},{3,27},{4,100},{5,29},{6,102},{7,31},{8,104},... | collective-permute-start | bytes 589832 | tf_op jit(solution)/shard_map/ppermute | solution.py:54
  44.9 6.1 %collective-permute-start.13 = (bf16[88,512]{1,0:T(8,128)(2,1)S(1)}, bf16[88,512]{1,0:T(8,128)(2,1)S(1)}, u32[]{:S(2)}, u32[]{:S(2)}) collective-permute-start(bf16[88,512]{1,0:T(8,128)(2,1)S(1)} %shard_map.101.refs_0_), channel_id=1, source_target_pairs={{0,16},{1,65},{2,18},{3,67},{4,20},{5,69},{6,22},{7,71},{8,24},{9,... | collective-permute-start | bytes 270344 | tf_op jit(solution)/shard_map/ppermute | solution.py:54
  47.6 6.4 %collective-permute-start.14 = (bf16[88,512]{1,0:T(8,128)(2,1)S(1)}, bf16[88,512]{1,0:T(8,128)(2,1)S(1)}, u32[]{:S(2)}, u32[]{:S(2)}) collective-permute-start(bf16[88,512]{1,0:T(8,128)(2,1)S(1)} %shard_map.101.refs_0_), channel_id=1, source_target_pairs={{0,24},{1,97},{2,26},{3,99},{4,28},{5,101},{6,30},{7,103},{8,16},{... | collective-permute-start | bytes 270344 | tf_op jit(solution)/shard_map/ppermute | solution.py:54
  54.9 5.3 %collective-permute-start.15 = (bf16[256,512]{1,0:T(8,128)(2,1)S(1)}, bf16[256,512]{1,0:T(8,128)(2,1)S(1)}, u32[]{:S(2)}, u32[]{:S(2)}) collective-permute-start(bf16[256,512]{1,0:T(8,128)(2,1)S(1)} %get-tuple-element.76), channel_id=1, source_target_pairs={{0,32},{1,9},{2,34},{3,11},{4,36},{5,13},{6,38},{7,15},{8,40},{9,1... | collective-permute-start | bytes 786440 | tf_op jit(solution)/shard_map/ppermute | solution.py:54
  55.0 8.9 %collective-permute-start.16 = (bf16[256,512]{1,0:T(8,128)(2,1)S(1)}, bf16[256,512]{1,0:T(8,128)(2,1)S(1)}, u32[]{:S(2)}, u32[]{:S(2)}) collective-permute-start(bf16[256,512]{1,0:T(8,128)(2,1)S(1)} %get-tuple-element.77), channel_id=1, source_target_pairs={{0,64},{1,17},{2,66},{3,19},{4,68},{5,21},{6,70},{7,23},{8,72},{9,... | collective-permute-start | bytes 786440 | tf_op jit(solution)/shard_map/ppermute | solution.py:54
  57.2 9.5 %collective-permute-start.17 = (bf16[256,512]{1,0:T(8,128)(2,1)S(1)}, bf16[256,512]{1,0:T(8,128)(2,1)S(1)}, u32[]{:S(2)}, u32[]{:S(2)}) collective-permute-start(bf16[256,512]{1,0:T(8,128)(2,1)S(1)} %get-tuple-element.78), channel_id=1, source_target_pairs={{0,96},{1,25},{2,98},{3,27},{4,100},{5,29},{6,102},{7,31},{8,104},... | collective-permute-start | bytes 786440 | tf_op jit(solution)/shard_map/ppermute | solution.py:54
  66.8 7.4 %collective-permute-start.18 = (bf16[256,256]{1,0:T(8,128)(2,1)S(1)}, bf16[256,256]{1,0:T(8,128)(2,1)S(1)}, u32[]{:S(2)}, u32[]{:S(2)}) collective-permute-start(bf16[256,256]{1,0:T(8,128)(2,1)S(1)} %get-tuple-element.80), channel_id=1, source_target_pairs={{0,1},{1,0},{2,3},{3,2},{4,5},{5,4},{6,7},{7,6},{8,9},{9,8},{10,11... | collective-permute-start | bytes 393224 | tf_op jit(solution)/shard_map/ppermute | solution.py:36
  70.4 25.5 %collective-permute-start.25 = (bf16[1408,256]{1,0:T(8,128)(2,1)S(1)}, bf16[1408,256]{1,0:T(8,128)(2,1)S(1)}, u32[]{:S(2)}, u32[]{:S(2)}) collective-permute-start(bf16[1408,256]{1,0:T(8,128)(2,1)S(1)} %get-tuple-element.86), channel_id=1, source_target_pairs={{0,32},{1,9},{2,34},{3,11},{4,36},{5,13},{6,38},{7,15},{8,40},{9,1... | collective-permute-start | bytes 2162696 | tf_op jit(solution)/shard_map/ppermute | solution.py:54
  70.4 25.5 %collective-permute-start.26 = (bf16[1408,256]{1,0:T(8,128)(2,1)S(1)}, bf16[1408,256]{1,0:T(8,128)(2,1)S(1)}, u32[]{:S(2)}, u32[]{:S(2)}) collective-permute-start(bf16[1408,256]{1,0:T(8,128)(2,1)S(1)} %get-tuple-element.87), channel_id=1, source_target_pairs={{0,64},{1,17},{2,66},{3,19},{4,68},{5,21},{6,70},{7,23},{8,72},{9,... | collective-permute-start | bytes 2162696 | tf_op jit(solution)/shard_map/ppermute | solution.py:54
  72.4 23.5 %collective-permute-start.27 = (bf16[1408,256]{1,0:T(8,128)(2,1)S(1)}, bf16[1408,256]{1,0:T(8,128)(2,1)S(1)}, u32[]{:S(2)}, u32[]{:S(2)}) collective-permute-start(bf16[1408,256]{1,0:T(8,128)(2,1)S(1)} %get-tuple-element.88), channel_id=1, source_target_pairs={{0,96},{1,25},{2,98},{3,27},{4,100},{5,29},{6,102},{7,31},{8,104},... | collective-permute-start | bytes 2162696 | tf_op jit(solution)/shard_map/ppermute | solution.py:54
  74.3 11.7 %copy-start.4 = (f32[2,256]{1,0:T(2,128)S(1)}, f32[2,256]{1,0:T(2,128)}, u32[]{:S(2)}) copy-start(f32[2,256]{1,0:T(2,128)} %gain.3) | copy-start | bytes 6148
  74.3 4.2 %collective-permute-start.19 = (bf16[256,256]{1,0:T(8,128)(2,1)S(1)}, bf16[256,256]{1,0:T(8,128)(2,1)S(1)}, u32[]{:S(2)}, u32[]{:S(2)}) collective-permute-start(bf16[256,256]{1,0:T(8,128)(2,1)S(1)} %shard_map.105.a), channel_id=1, source_target_pairs={{0,2},{1,3},{2,0},{3,1},{4,6},{5,7},{6,4},{7,5},{8,10},{9,11},{10,... | collective-permute-start | bytes 393224 | tf_op jit(solution)/shard_map/ppermute | solution.py:54
  75.6 7.9 %collective-permute-start.20 = (bf16[256,256]{1,0:T(8,128)(2,1)S(1)}, bf16[256,256]{1,0:T(8,128)(2,1)S(1)}, u32[]{:S(2)}, u32[]{:S(2)}) collective-permute-start(bf16[256,256]{1,0:T(8,128)(2,1)S(1)} %shard_map.105.a), channel_id=1, source_target_pairs={{0,4},{1,5},{2,6},{3,7},{4,0},{5,1},{6,2},{7,3},{8,12},{9,13},{10,... | collective-permute-start | bytes 393224 | tf_op jit(solution)/shard_map/ppermute | solution.py:54
  78.5 7.5 %collective-permute-start.21 = (bf16[256,256]{1,0:T(8,128)(2,1)S(1)}, bf16[256,256]{1,0:T(8,128)(2,1)S(1)}, u32[]{:S(2)}, u32[]{:S(2)}) collective-permute-start(bf16[256,256]{1,0:T(8,128)(2,1)S(1)} %shard_map.105.a), channel_id=1, source_target_pairs={{0,6},{1,7},{2,4},{3,5},{4,2},{5,3},{6,0},{7,1},{8,14},{9,15},{10,... | collective-permute-start | bytes 393224 | tf_op jit(solution)/shard_map/ppermute | solution.py:54
  86.2 4.3 %collective-permute-start.28 = (bf16[272,256]{1,0:T(8,128)(2,1)S(1)}, bf16[272,256]{1,0:T(8,128)(2,1)S(1)}, u32[]{:S(2)}, u32[]{:S(2)}) collective-permute-start(bf16[272,256]{1,0:T(8,128)(2,1)S(1)} %get-tuple-element.82.refs_4_), channel_id=1, source_target_pairs={{0,32},{1,9},{2,34},{3,11},{4,36},{5,13},{6,38},{7,15},{8,40},{9,1... | collective-permute-start | bytes 417800 | tf_op jit(solution)/shard_map/ppermute | solution.py:54
  86.3 6.0 %collective-permute-start.29 = (bf16[272,256]{1,0:T(8,128)(2,1)S(1)}, bf16[272,256]{1,0:T(8,128)(2,1)S(1)}, u32[]{:S(2)}, u32[]{:S(2)}) collective-permute-start(bf16[272,256]{1,0:T(8,128)(2,1)S(1)} %get-tuple-element.82.refs_4_), channel_id=1, source_target_pairs={{0,64},{1,17},{2,66},{3,19},{4,68},{5,21},{6,70},{7,23},{8,72},{9,... | collective-permute-start | bytes 417800 | tf_op jit(solution)/shard_map/ppermute | solution.py:54
  90.5 5.4 %collective-permute-start.30 = (bf16[272,256]{1,0:T(8,128)(2,1)S(1)}, bf16[272,256]{1,0:T(8,128)(2,1)S(1)}, u32[]{:S(2)}, u32[]{:S(2)}) collective-permute-start(bf16[272,256]{1,0:T(8,128)(2,1)S(1)} %get-tuple-element.82.refs_4_), channel_id=1, source_target_pairs={{0,96},{1,25},{2,98},{3,27},{4,100},{5,29},{6,102},{7,31},{8,104},... | collective-permute-start | bytes 417800 | tf_op jit(solution)/shard_map/ppermute | solution.py:54
  97.0 6.0 %collective-permute-start.31 = (bf16[368,256]{1,0:T(8,128)(2,1)S(1)}, bf16[368,256]{1,0:T(8,128)(2,1)S(1)}, u32[]{:S(2)}, u32[]{:S(2)}) collective-permute-start(bf16[368,256]{1,0:T(8,128)(2,1)S(1)} %get-tuple-element.90), channel_id=1, source_target_pairs={{0,8},{1,33},{2,10},{3,35},{4,12},{5,37},{6,14},{7,39},{8,0},{9,41... | collective-permute-start | bytes 565256 | tf_op jit(solution)/shard_map/ppermute | solution.py:54
  97.1 8.5 %collective-permute-start.32 = (bf16[368,256]{1,0:T(8,128)(2,1)S(1)}, bf16[368,256]{1,0:T(8,128)(2,1)S(1)}, u32[]{:S(2)}, u32[]{:S(2)}) collective-permute-start(bf16[368,256]{1,0:T(8,128)(2,1)S(1)} %get-tuple-element.91), channel_id=1, source_target_pairs={{0,16},{1,65},{2,18},{3,67},{4,20},{5,69},{6,22},{7,71},{8,24},{9,... | collective-permute-start | bytes 565256 | tf_op jit(solution)/shard_map/ppermute | solution.py:54
  100.5 7.3 %collective-permute-start.33 = (bf16[368,256]{1,0:T(8,128)(2,1)S(1)}, bf16[368,256]{1,0:T(8,128)(2,1)S(1)}, u32[]{:S(2)}, u32[]{:S(2)}) collective-permute-start(bf16[368,256]{1,0:T(8,128)(2,1)S(1)} %get-tuple-element.92), channel_id=1, source_target_pairs={{0,24},{1,97},{2,26},{3,99},{4,28},{5,101},{6,30},{7,103},{8,16},{... | collective-permute-start | bytes 565256 | tf_op jit(solution)/shard_map/ppermute | solution.py:54
  100.9 22.1 %collective-permute-start.22 = (bf16[256,768]{1,0:T(8,128)(2,1)S(1)}, bf16[256,768]{1,0:T(8,128)(2,1)S(1)}, u32[]{:S(2)}, u32[]{:S(2)}) collective-permute-start(bf16[256,768]{1,0:T(8,128)(2,1)S(1)} %get-tuple-element.83), channel_id=1, source_target_pairs={{0,32},{1,9},{2,34},{3,11},{4,36},{5,13},{6,38},{7,15},{8,40},{9,1... | collective-permute-start | bytes 1179656 | tf_op jit(solution)/shard_map/ppermute | solution.py:54
  100.9 22.1 %collective-permute-start.23 = (bf16[256,768]{1,0:T(8,128)(2,1)S(1)}, bf16[256,768]{1,0:T(8,128)(2,1)S(1)}, u32[]{:S(2)}, u32[]{:S(2)}) collective-permute-start(bf16[256,768]{1,0:T(8,128)(2,1)S(1)} %get-tuple-element.84), channel_id=1, source_target_pairs={{0,64},{1,17},{2,66},{3,19},{4,68},{5,21},{6,70},{7,23},{8,72},{9,... | collective-permute-start | bytes 1179656 | tf_op jit(solution)/shard_map/ppermute | solution.py:54
  103.0 20.1 %collective-permute-start.24 = (bf16[256,768]{1,0:T(8,128)(2,1)S(1)}, bf16[256,768]{1,0:T(8,128)(2,1)S(1)}, u32[]{:S(2)}, u32[]{:S(2)}) collective-permute-start(bf16[256,768]{1,0:T(8,128)(2,1)S(1)} %get-tuple-element.85), channel_id=1, source_target_pairs={{0,96},{1,25},{2,98},{3,27},{4,100},{5,29},{6,102},{7,31},{8,104},... | collective-permute-start | bytes 1179656 | tf_op jit(solution)/shard_map/ppermute | solution.py:54
  108.4 4.7 %collective-permute-start.34 = (bf16[176,256]{1,0:T(8,128)(2,1)S(1)}, bf16[176,256]{1,0:T(8,128)(2,1)S(1)}, u32[]{:S(2)}, u32[]{:S(2)}) collective-permute-start(bf16[176,256]{1,0:T(8,128)(2,1)S(1)} %shard_map.108.refs_0_), channel_id=1, source_target_pairs={{0,8},{1,33},{2,10},{3,35},{4,12},{5,37},{6,14},{7,39},{8,0},{9,41... | collective-permute-start | bytes 270344 | tf_op jit(solution)/shard_map/ppermute | solution.py:54
  108.5 6.1 %collective-permute-start.35 = (bf16[176,256]{1,0:T(8,128)(2,1)S(1)}, bf16[176,256]{1,0:T(8,128)(2,1)S(1)}, u32[]{:S(2)}, u32[]{:S(2)}) collective-permute-start(bf16[176,256]{1,0:T(8,128)(2,1)S(1)} %shard_map.108.refs_0_), channel_id=1, source_target_pairs={{0,16},{1,65},{2,18},{3,67},{4,20},{5,69},{6,22},{7,71},{8,24},{9,... | collective-permute-start | bytes 270344 | tf_op jit(solution)/shard_map/ppermute | solution.py:54
  113.2 9.7 %collective-permute-start.36 = (bf16[176,256]{1,0:T(8,128)(2,1)S(1)}, bf16[176,256]{1,0:T(8,128)(2,1)S(1)}, u32[]{:S(2)}, u32[]{:S(2)}) collective-permute-start(bf16[176,256]{1,0:T(8,128)(2,1)S(1)} %shard_map.108.refs_0_), channel_id=1, source_target_pairs={{0,24},{1,97},{2,26},{3,99},{4,28},{5,101},{6,30},{7,103},{8,16},{... | collective-permute-start | bytes 270344 | tf_op jit(solution)/shard_map/ppermute | solution.py:54
  123.7 4.2 %collective-permute-start.37 = (bf16[256,256]{1,0:T(8,128)(2,1)S(1)}, bf16[256,256]{1,0:T(8,128)(2,1)S(1)}, u32[]{:S(2)}, u32[]{:S(2)}) collective-permute-start(bf16[256,256]{1,0:T(8,128)(2,1)S(1)} %get-tuple-element.94), channel_id=1, source_target_pairs={{0,32},{1,9},{2,34},{3,11},{4,36},{5,13},{6,38},{7,15},{8,40},{9,1... | collective-permute-start | bytes 393224 | tf_op jit(solution)/shard_map/ppermute | solution.py:54
  123.8 5.7 %collective-permute-start.38 = (bf16[256,256]{1,0:T(8,128)(2,1)S(1)}, bf16[256,256]{1,0:T(8,128)(2,1)S(1)}, u32[]{:S(2)}, u32[]{:S(2)}) collective-permute-start(bf16[256,256]{1,0:T(8,128)(2,1)S(1)} %get-tuple-element.95), channel_id=1, source_target_pairs={{0,64},{1,17},{2,66},{3,19},{4,68},{5,21},{6,70},{7,23},{8,72},{9,... | collective-permute-start | bytes 393224 | tf_op jit(solution)/shard_map/ppermute | solution.py:54
  125.7 5.4 %collective-permute-start.39 = (bf16[256,256]{1,0:T(8,128)(2,1)S(1)}, bf16[256,256]{1,0:T(8,128)(2,1)S(1)}, u32[]{:S(2)}, u32[]{:S(2)}) collective-permute-start(bf16[256,256]{1,0:T(8,128)(2,1)S(1)} %get-tuple-element.96), channel_id=1, source_target_pairs={{0,96},{1,25},{2,98},{3,27},{4,100},{5,29},{6,102},{7,31},{8,104},... | collective-permute-start | bytes 393224 | tf_op jit(solution)/shard_map/ppermute | solution.py:54
  131.2 4.2 %collective-permute-start.40 = (bf16[256,256]{1,0:T(8,128)(2,1)S(1)}, bf16[256,256]{1,0:T(8,128)(2,1)S(1)}, u32[]{:S(2)}, u32[]{:S(2)}) collective-permute-start(bf16[256,256]{1,0:T(8,128)(2,1)S(1)} %shard_map.111.a), channel_id=1, source_target_pairs={{0,2},{1,3},{2,0},{3,1},{4,6},{5,7},{6,4},{7,5},{8,10},{9,11},{10,... | collective-permute-start | bytes 393224 | tf_op jit(solution)/shard_map/ppermute | solution.py:54
  131.3 8.0 %collective-permute-start.41 = (bf16[256,256]{1,0:T(8,128)(2,1)S(1)}, bf16[256,256]{1,0:T(8,128)(2,1)S(1)}, u32[]{:S(2)}, u32[]{:S(2)}) collective-permute-start(bf16[256,256]{1,0:T(8,128)(2,1)S(1)} %shard_map.111.a), channel_id=1, source_target_pairs={{0,4},{1,5},{2,6},{3,7},{4,0},{5,1},{6,2},{7,3},{8,12},{9,13},{10,... | collective-permute-start | bytes 393224 | tf_op jit(solution)/shard_map/ppermute | solution.py:54
  135.2 5.5 %collective-permute-start.42 = (bf16[256,256]{1,0:T(8,128)(2,1)S(1)}, bf16[256,256]{1,0:T(8,128)(2,1)S(1)}, u32[]{:S(2)}, u32[]{:S(2)}) collective-permute-start(bf16[256,256]{1,0:T(8,128)(2,1)S(1)} %shard_map.111.a), channel_id=1, source_target_pairs={{0,6},{1,7},{2,4},{3,5},{4,2},{5,3},{6,0},{7,1},{8,14},{9,15},{10,... | collective-permute-start | bytes 393224 | tf_op jit(solution)/shard_map/ppermute | solution.py:54
  140.8 13.1 %collective-permute-start.43 = (bf16[2,128,256]{2,1,0:T(8,128)(2,1)S(1)}, bf16[2,128,256]{2,1,0:T(8,128)(2,1)S(1)}, u32[]{:S(2)}, u32[]{:S(2)}) collective-permute-start(bf16[2,128,256]{2,1,0:T(8,128)(2,1)S(1)} %shard_map.112.mine), channel_id=1, source_target_pairs={{0,1},{1,0},{2,3},{3,2},{4,5},{5,4},{6,7},{7,6},{8,9},{9,8},{10,11... | collective-permute-start | bytes 393224 | tf_op jit(solution)/shard_map/ppermute | solution.py:36
where the time goes:
time: 155 us
  waiting for transfers between devices  73 us (47%)
  starting transfers between devices  68 us (44%)
  Pallas kernels  13.2 us (9%)
    ppermute x39, waiting for transfers between devices, moved(): got[d] = lax.ppermute(values[d], AXES, pairs(move(d)))  72 us
    ppermute x39, starting transfers between devices, moved(): got[d] = lax.ppermute(values[d], AXES, pairs(move(d)))  50.2 us
    ppermute x5, starting transfers between devices, to_twin(): return lax.ppermute(value, AXES, pairs(lambda z, y, x, c: (z, y, x, 1 - c)))  17.8 us
    pallas_call x23, Pallas kernels, local(): pl.pallas_call(kernel, in_specs=specs or [VMEM] * len(args), out_specs=[V...  13.2 us
  transfers between devices with their start and end apart: 44, of which 28 were waited for; matrix products, arithmetic and copies ran while one was open for 0% of the time, Pallas kernels for 4%

commit v1 on v0

--- a/solution.py
+++ b/solution.py
@@ -10,7 +10,7 @@
 KERNEL = 3
 LAYERS = 2
 SIDE = 4
-EXTRA = 16
+EXTRA = 8
 AXES = ("ra", "cb")
 BF16 = jnp.bfloat16
 F32 = jnp.float32
@@ -298,21 +298,42 @@
     return local(kernel, array((2 * seqs, length, width), BF16), mine, other)
 
 
-def products(unit, width, rows, operands, read, order):
+def accumulated(ins, read, h, total, squares):
+    for weights, acts, extra in read(ins, h):
+        total = total + jnp.dot(weights, acts, preferred_element_type=F32)
+        extra = extra.astype(F32)
+        squares = squares + extra[0:1] + extra[1:2]
+    return total, squares
+
+
+def begun(rows, operands, read):
+    stretches, count, step = rows
+    tokens = stretches * step
+
+    def kernel(*refs):
+        ins, (total, squares) = refs[:-2], refs[-2:]
+        for h in range(stretches):
+            cut = slice(h * step, (h + 1) * step)
+            total[:, cut], row = accumulated(ins, read, h, 0.0, 0.0)
+            squares[:, cut] = jnp.broadcast_to(row, (8, step))
+
+    outs = [array((count, tokens), F32), array((8, tokens), F32)]
+    return local(kernel, outs, *operands)
+
+
+def products(unit, width, rows, begin_with, operands, read, order):
     share = unit // SIDE
     stretches, count, step = rows
+    n = len(operands)
 
     def kernel(*refs):
-        ins, outs, acc = refs[: len(operands)], refs[len(operands) : -1], refs[-1]
+        ins, (start_total, start_squares), outs, acc = refs[:n], refs[n : n + 2], refs[n + 2 : -1], refs[-1]
         _, _, second = position()
         for h in range(stretches):
             cut = slice(h * step, (h + 1) * step)
-            total, squares = 0.0, 0.0
-            for weights, acts, extra in read(ins, h):
-                total = total + jnp.dot(weights, acts, preferred_element_type=F32)
-                extra = extra.astype(F32)
-                squares = squares + extra[0:1] + extra[1:2]
-            acc[:, cut] = total
+            acc[:, cut], squares = accumulated(
+                ins, read, h, start_total[:, cut], start_squares[0:1, cut]
+            )
             squares = split_rows(squares)
             for out in outs:
                 out[count // SIDE :, cut] = squares
@@ -326,13 +347,15 @@
         kernel,
         [array((count // SIDE + EXTRA, tokens), BF16)] * len(order),
         *operands,
+        *begin_with,
         flops=2 * count * SIDE * width * tokens,
         scratch=[pltpu.VMEM((count, tokens), F32)],
     )
 
 
-def first_products(packs, unit, width, half, order):
+def first_products(own, packs, unit, width, half, order):
     count = 2 * unit
+    rows = (2, count, half)
 
     def read(refs, h):
         start = count + h * (width + EXTRA)
@@ -340,17 +363,20 @@
             acts = ref[start : start + width]
             yield ref[:count], acts, ref[start + width : start + width + EXTRA]
 
-    return products(unit, width, (2, count, half), packs, read, order)
-
-
-def next_products(weights, acts, unit, width, half, order):
-    n = len(weights)
+    begin_with = begun(rows, [own], read)
+    return products(unit, width, rows, begin_with, packs, read, order)
+
+
+def next_products(own, weights, acts, unit, width, half, order):
+    rows = (1, 4 * unit, half)
 
     def read(refs, h):
+        n = len(refs) // 2
         for w, a in zip(refs[:n], refs[n:]):
             yield w[...], a[:width], a[width:]
 
-    return products(unit, width, (1, 4 * unit, half), [*weights, *acts], read, order)
+    begin_with = begun(rows, own, read)
+    return products(unit, width, rows, begin_with, [*weights, *acts], read, order)
 
 
 def gated(parts, small, which, share, length):
@@ -481,19 +507,20 @@
     small = turn_small(small, to_twin(small))
     got = moved(first_move, packs)
     got = after(got, downs, turned, small)
-    got = [packs[0], *(got[d] for d in every[1:])]
+    got = [got[d] for d in every[1:]]
     late = moved(first_move, downs[0])
     late = [downs[0][0], late[1], late[2], late[3]]
-    parts = first_products(got, unit, width, half, every)
+    parts = first_products(packs[0], got, unit, width, half, every)
     for l in range(LAYERS):
         got = moved(second_move, parts)
         which = (0,) if l == 0 else (1, LAYERS + 1)
         hidden = gated([parts[0], got[1], got[2], got[3]], small, which, share, length)
         got = moved(second_move, [hidden] * SIDE)
         block = collected([hidden, got[1], got[2], got[3]], share, every)
-        branch = spread(late, range(l + 1), lanes, block)
-        got = moved(first_move, branch)
-        got = [branch[0], got[1], got[2], got[3]]
+        branch = [spread([w], range(l + 1), lanes, block)[0] for w in late[1:]]
+        got = moved(first_move, [None, *branch])
+        (mine,) = spread(late[:1], range(l + 1), lanes, block)
+        got = [mine, got[1], got[2], got[3]]
         if l == 0:
             weights = moved(first_move, after(turned, block))
             weights = [turned[0], weights[1], weights[2], weights[3]]
@@ -506,10 +533,11 @@
         if l == 0:
             carried, acts = next_block(carried, got, norm_gain, l + 1)
             got = moved(first_move, [acts] * SIDE)
-            got = [acts, got[1], got[2], got[3]]
+            got = [got[1], got[2], got[3]]
             late = moved(first_move, after(downs[1], acts))
             late = [downs[1][0], late[1], late[2], late[3]]
-            parts = next_products(weights, got, unit, width, half, every)
+            own = [weights[0], acts]
+            parts = next_products(own, weights[1:], got, unit, width, half, every)
     mine = last_block(carried, got, seqs // 2, length)
     return joined(mine, to_twin(mine))
 

time: 155 us -> 154 us (level)
  waiting for transfers between devices: 73 us -> 69.4 us
    ppermute x39, waiting for transfers between devices: 72 us -> 68.4 us  [moved(): got[d] = lax.ppermute(values[d], AXES, pairs(move(d)))]
    pallas_call x23 -> x31, Pallas kernels: 13.2 us -> 14.5 us  [local(): pl.pallas_call(kernel, in_specs=specs or [VMEM] * len(args), out_specs=[V...]
  transfers between devices with their start and end apart: 44 -> 44, of which waited for: 28 -> 25; matrix products, arithmetic and copies ran while one was open for 0% -> 0% of each run, Pallas kernels for 4% -> 6%
where the time goes in v1:
time: 154 us
  waiting for transfers between devices  69.4 us (45%)
  starting transfers between devices  69.3 us (45%)
  Pallas kernels  14.5 us (9%)
    ppermute x39, waiting for transfers between devices, moved(): got[d] = lax.ppermute(values[d], AXES, pairs(move(d)))  68.4 us
    ppermute x39, starting transfers between devices, moved(): got[d] = lax.ppermute(values[d], AXES, pairs(move(d)))  49.9 us
    ppermute x5, starting transfers between devices, to_twin(): return lax.ppermute(value, AXES, pairs(lambda z, y, x, c: (z, y, x, 1 - c)))  19.3 us
    pallas_call x31, Pallas kernels, local(): pl.pallas_call(kernel, in_specs=specs or [VMEM] * len(args), out_specs=[V...  14.5 us
  transfers between devices with their start and end apart: 44, of which 25 were waited for; matrix products, arithmetic and copies ran while one was open for 0% of the time, Pallas kernels for 6%

profile of v1, /device:TPU:1, one launch (start us, length us, event | category | flops | bytes accessed | tf_op | source)
XLA Modules:
  0.0 153.6 jit_solution(16180832708144934059)
XLA Ops:
  0.0 1.6 %shard_map.96.mine = bf16[2816,256]{1,0:T(8,128)(2,1)S(1)} custom-call(bf16[2,256,1408]{2,1,0:T(8,128)(2,1)} %gate.3, bf16[2,256,1408]{2,1,0:T(8,128)(2,1)} %up.3), custom_call_target="tpu_custom_call" | custom-call | flops 1000000000 | bytes 2883584 | tf_op jit(solution)/shard_map/pallas_call | solution.py:71
  1.7 1.5 collective-permute-start.4
  3.2 1.4 shard_map.94.refs_0_
  4.7 0.5 collective-permute-start.5
  5.3 1.9 %shard_map.91 = (bf16[1232,256]{1,0:T(8,128)(2,1)S(1)}, bf16[1232,256]{1,0:T(8,128)(2,1)S(1)}, bf16[1232,256]{1,0:T(8,128)(2,1)S(1)}, bf16[1232,256]{1,0:T(8,128)(2,1)S(1)}, f32[256,256]{1,0:T(8,128)S(1)}) custom-call(bf16[4,128,256]{2,1,0:T(8,128)(2,1)} %tokens.1, f32[2,256]{1,0:T(2,128)} %gain.3, bf16[2,256,1408]{2,1,0:T(8,128)(2,1)} %gate.3, ...), custom_call_target="tpu_custom_call" | custom-call | flops 1000000000 | bytes 3147776 | tf_op jit(solution)/shard_map/pallas_call | solution.py:71
  7.2 1.5 collective-permute-start
  8.7 2.6 %collective-permute-start.1 = (bf16[1232,256]{1,0:T(8,128)(2,1)S(1)}, bf16[1232,256]{1,0:T(8,128)(2,1)S(1)}, u32[]{:S(2)}, u32[]{:S(2)}) collective-permute-start(bf16[1232,256]{1,0:T(8,128)(2,1)S(1)} %get-tuple-element.50), channel_id=1, source_target_pairs={{0,64},{1,17},{2,66},{3,19},{4,68},{5,21},{6,70},{7,23},{8,72},{9,... | collective-permute-start | bytes 1892360 | tf_op jit(solution)/shard_map/ppermute | solution.py:54
  11.3 1.4 shard_map.92.refs_0_
  12.8 0.3 shard_map.100
  13.8 2.9 %collective-permute-done.refs_0_ = bf16[1232,256]{1,0:T(8,128)(2,1)S(1)} collective-permute-done((bf16[1232,256]{1,0:T(8,128)(2,1)S(1)}, bf16[1232,256]{1,0:T(8,128)(2,1)S(1)}, u32[]{:S(2)}, u32[]{:S(2)}) %collective-permute-start) | collective-permute-done | bytes 630816 | tf_op jit(solution)/shard_map/ppermute | solution.py:54
  16.8 9.4 %collective-permute-done.1.refs_1_ = bf16[1232,256]{1,0:T(8,128)(2,1)S(1)} collective-permute-done((bf16[1232,256]{1,0:T(8,128)(2,1)S(1)}, bf16[1232,256]{1,0:T(8,128)(2,1)S(1)}, u32[]{:S(2)}, u32[]{:S(2)}) %collective-permute-start.1) | collective-permute-done | bytes 630816 | tf_op jit(solution)/shard_map/ppermute | solution.py:54
  26.1 2.6 %collective-permute-done.2.refs_2_ = bf16[1232,256]{1,0:T(8,128)(2,1)S(1)} collective-permute-done((bf16[1232,256]{1,0:T(8,128)(2,1)S(1)}, bf16[1232,256]{1,0:T(8,128)(2,1)S(1)}, u32[]{:S(2)}, u32[]{:S(2)}) %collective-permute-start.2) | collective-permute-done | bytes 630816 | tf_op jit(solution)/shard_map/ppermute | solution.py:54
  28.8 0.8 shard_map.101
  29.6 1.4 collective-permute-start.6
  31.0 3.3 %collective-permute-start.7 = (bf16[184,512]{1,0:T(8,128)(2,1)S(1)}, bf16[184,512]{1,0:T(8,128)(2,1)S(1)}, u32[]{:S(2)}, u32[]{:S(2)}) collective-permute-start(bf16[184,512]{1,0:T(8,128)(2,1)S(1)} %get-tuple-element.71), channel_id=1, source_target_pairs={{0,16},{1,65},{2,18},{3,67},{4,20},{5,69},{6,22},{7,71},{8,24},{9,... | collective-permute-start | bytes 565256 | tf_op jit(solution)/shard_map/ppermute | solution.py:54
  34.3 5.1 %collective-permute-done.7.c = bf16[184,512]{1,0:T(8,128)(2,1)S(1)} collective-permute-done((bf16[184,512]{1,0:T(8,128)(2,1)S(1)}, bf16[184,512]{1,0:T(8,128)(2,1)S(1)}, u32[]{:S(2)}, u32[]{:S(2)}) %collective-permute-start.7) | collective-permute-done | bytes 188448 | tf_op jit(solution)/shard_map/ppermute | solution.py:54
  39.4 2.2 %collective-permute-done.8.d = bf16[184,512]{1,0:T(8,128)(2,1)S(1)} collective-permute-done((bf16[184,512]{1,0:T(8,128)(2,1)S(1)}, bf16[184,512]{1,0:T(8,128)(2,1)S(1)}, u32[]{:S(2)}, u32[]{:S(2)}) %collective-permute-start.8) | collective-permute-done | bytes 188448 | tf_op jit(solution)/shard_map/ppermute | solution.py:54
  41.6 0.6 shard_map.102.refs_0_
  42.4 1.5 collective-permute-start.14
  43.9 0.6 collective-permute-start.10
  44.5 2.5 %collective-permute-start.9 = (bf16[88,512]{1,0:T(8,128)(2,1)S(1)}, bf16[88,512]{1,0:T(8,128)(2,1)S(1)}, u32[]{:S(2)}, u32[]{:S(2)}) collective-permute-start(bf16[88,512]{1,0:T(8,128)(2,1)S(1)} %shard_map.102.refs_0_), channel_id=1, source_target_pairs={{0,8},{1,33},{2,10},{3,35},{4,12},{5,37},{6,14},{7,39},{8,0},{9,41... | collective-permute-start | bytes 270344 | tf_op jit(solution)/shard_map/ppermute | solution.py:54
  47.1 2.4 %collective-permute-start.16 = (bf16[256,384]{1,0:T(8,128)(2,1)S(1)}, bf16[256,384]{1,0:T(8,128)(2,1)S(1)}, u32[]{:S(2)}, u32[]{:S(2)}) collective-permute-start(bf16[256,384]{1,0:T(8,128)(2,1)S(1)} %get-tuple-element.54), channel_id=1, source_target_pairs={{0,96},{1,25},{2,98},{3,27},{4,100},{5,29},{6,102},{7,31},{8,104},... | collective-permute-start | bytes 589832 | tf_op jit(solution)/shard_map/ppermute | solution.py:54
  49.5 2.0 %collective-permute-done.9.refs_1_ = bf16[88,512]{1,0:T(8,128)(2,1)S(1)} collective-permute-done((bf16[88,512]{1,0:T(8,128)(2,1)S(1)}, bf16[88,512]{1,0:T(8,128)(2,1)S(1)}, u32[]{:S(2)}, u32[]{:S(2)}) %collective-permute-start.9) | collective-permute-done | bytes 90144 | tf_op jit(solution)/shard_map/ppermute | solution.py:54
  51.7 0.3 shard_map.105
  52.0 0.5 collective-permute-start.13
  52.5 0.3 shard_map.106
  52.8 3.4 %collective-permute-start.15 = (bf16[256,512]{1,0:T(8,128)(2,1)S(1)}, bf16[256,512]{1,0:T(8,128)(2,1)S(1)}, u32[]{:S(2)}, u32[]{:S(2)}) collective-permute-start(bf16[256,512]{1,0:T(8,128)(2,1)S(1)} %shard_map.106), channel_id=1, source_target_pairs={{0,64},{1,17},{2,66},{3,19},{4,68},{5,21},{6,70},{7,23},{8,72},{9,... | collective-permute-start | bytes 786440 | tf_op jit(solution)/shard_map/ppermute | solution.py:54
  56.2 0.3 shard_map.107
  56.8 0.3 shard_map.104.a
  57.3 5.2 %collective-permute-done.15.c = bf16[256,512]{1,0:T(8,128)(2,1)S(1)} collective-permute-done((bf16[256,512]{1,0:T(8,128)(2,1)S(1)}, bf16[256,512]{1,0:T(8,128)(2,1)S(1)}, u32[]{:S(2)}, u32[]{:S(2)}) %collective-permute-start.15) | collective-permute-done | bytes 262176 | tf_op jit(solution)/shard_map/ppermute | solution.py:54
  62.5 3.0 %collective-permute-done.17.d = bf16[256,512]{1,0:T(8,128)(2,1)S(1)} collective-permute-done((bf16[256,512]{1,0:T(8,128)(2,1)S(1)}, bf16[256,512]{1,0:T(8,128)(2,1)S(1)}, u32[]{:S(2)}, u32[]{:S(2)}) %collective-permute-start.17) | collective-permute-done | bytes 262176 | tf_op jit(solution)/shard_map/ppermute | solution.py:54
  65.6 5.0 %collective-permute-start.18 = (bf16[256,256]{1,0:T(8,128)(2,1)S(1)}, bf16[256,256]{1,0:T(8,128)(2,1)S(1)}, u32[]{:S(2)}, u32[]{:S(2)}) collective-permute-start(bf16[256,256]{1,0:T(8,128)(2,1)S(1)} %get-tuple-element.74), channel_id=1, source_target_pairs={{0,1},{1,0},{2,3},{3,2},{4,5},{5,4},{6,7},{7,6},{8,9},{9,8},{10,11... | collective-permute-start | bytes 393224 | tf_op jit(solution)/shard_map/ppermute | solution.py:36
  70.6 0.5 collective-permute-start.22
  71.0 1.2 collective-permute-start.23
  72.2 2.2 %collective-permute-start.24 = (bf16[1408,256]{1,0:T(8,128)(2,1)S(1)}, bf16[1408,256]{1,0:T(8,128)(2,1)S(1)}, u32[]{:S(2)}, u32[]{:S(2)}) collective-permute-start(bf16[1408,256]{1,0:T(8,128)(2,1)S(1)} %get-tuple-element.78), channel_id=1, source_target_pairs={{0,96},{1,25},{2,98},{3,27},{4,100},{5,29},{6,102},{7,31},{8,104},... | collective-permute-start | bytes 2162696 | tf_op jit(solution)/shard_map/ppermute | solution.py:54
  74.5 2.6 %collective-permute-start.21 = (bf16[256,256]{1,0:T(8,128)(2,1)S(1)}, bf16[256,256]{1,0:T(8,128)(2,1)S(1)}, u32[]{:S(2)}, u32[]{:S(2)}) collective-permute-start(bf16[256,256]{1,0:T(8,128)(2,1)S(1)} %shard_map.109.a), channel_id=1, source_target_pairs={{0,6},{1,7},{2,4},{3,5},{4,2},{5,3},{6,0},{7,1},{8,14},{9,15},{10,... | collective-permute-start | bytes 393224 | tf_op jit(solution)/shard_map/ppermute | solution.py:54
  77.0 0.5 collective-permute-start.20
  77.6 5.0 %collective-permute-done.21.d = bf16[256,256]{1,0:T(8,128)(2,1)S(1)} collective-permute-done((bf16[256,256]{1,0:T(8,128)(2,1)S(1)}, bf16[256,256]{1,0:T(8,128)(2,1)S(1)}, u32[]{:S(2)}, u32[]{:S(2)}) %collective-permute-start.21) | collective-permute-done | bytes 131104 | tf_op jit(solution)/shard_map/ppermute | solution.py:54
  82.7 4.0 %collective-permute-done.19.b = bf16[256,256]{1,0:T(8,128)(2,1)S(1)} collective-permute-done((bf16[256,256]{1,0:T(8,128)(2,1)S(1)}, bf16[256,256]{1,0:T(8,128)(2,1)S(1)}, u32[]{:S(2)}, u32[]{:S(2)}) %collective-permute-start.19) | collective-permute-done | bytes 131104 | tf_op jit(solution)/shard_map/ppermute | solution.py:54
  87.0 0.5 collective-permute-start.27
  87.5 7.0 %collective-permute-done.27.refs_5_ = bf16[264,256]{1,0:T(8,128)(2,1)S(1)} collective-permute-done((bf16[264,256]{1,0:T(8,128)(2,1)S(1)}, bf16[264,256]{1,0:T(8,128)(2,1)S(1)}, u32[]{:S(2)}, u32[]{:S(2)}) %collective-permute-start.27) | collective-permute-done | bytes 135200 | tf_op jit(solution)/shard_map/ppermute | solution.py:54
  94.5 0.3 shard_map.111
  94.9 3.5 %collective-permute-done.25.refs_3_ = bf16[264,256]{1,0:T(8,128)(2,1)S(1)} collective-permute-done((bf16[264,256]{1,0:T(8,128)(2,1)S(1)}, bf16[264,256]{1,0:T(8,128)(2,1)S(1)}, u32[]{:S(2)}, u32[]{:S(2)}) %collective-permute-start.25) | collective-permute-done | bytes 135200 | tf_op jit(solution)/shard_map/ppermute | solution.py:54
  98.4 0.9 shard_map.112
  99.3 1.1 collective-permute-start.29
  100.5 2.7 %collective-permute-start.30 = (bf16[360,256]{1,0:T(8,128)(2,1)S(1)}, bf16[360,256]{1,0:T(8,128)(2,1)S(1)}, u32[]{:S(2)}, u32[]{:S(2)}) collective-permute-start(bf16[360,256]{1,0:T(8,128)(2,1)S(1)} %get-tuple-element.85), channel_id=1, source_target_pairs={{0,24},{1,97},{2,26},{3,99},{4,28},{5,101},{6,30},{7,103},{8,16},{... | collective-permute-start | bytes 552968 | tf_op jit(solution)/shard_map/ppermute | solution.py:54
  103.2 3.6 %collective-permute-start.36 = (bf16[256,768]{1,0:T(8,128)(2,1)S(1)}, bf16[256,768]{1,0:T(8,128)(2,1)S(1)}, u32[]{:S(2)}, u32[]{:S(2)}) collective-permute-start(bf16[256,768]{1,0:T(8,128)(2,1)S(1)} %get-tuple-element.87), channel_id=1, source_target_pairs={{0,64},{1,17},{2,66},{3,19},{4,68},{5,21},{6,70},{7,23},{8,72},{9,... | collective-permute-start | bytes 1179656 | tf_op jit(solution)/shard_map/ppermute | solution.py:54
  107.3 0.6 shard_map.113.refs_0_
  107.9 2.8 %collective-permute-start.33 = (bf16[176,256]{1,0:T(8,128)(2,1)S(1)}, bf16[176,256]{1,0:T(8,128)(2,1)S(1)}, u32[]{:S(2)}, u32[]{:S(2)}) collective-permute-start(bf16[176,256]{1,0:T(8,128)(2,1)S(1)} %shard_map.113.refs_0_), channel_id=1, source_target_pairs={{0,24},{1,97},{2,26},{3,99},{4,28},{5,101},{6,30},{7,103},{8,16},{... | collective-permute-start | bytes 270344 | tf_op jit(solution)/shard_map/ppermute | solution.py:54
  110.8 2.2 %collective-permute-done.33.refs_3_ = bf16[176,256]{1,0:T(8,128)(2,1)S(1)} collective-permute-done((bf16[176,256]{1,0:T(8,128)(2,1)S(1)}, bf16[176,256]{1,0:T(8,128)(2,1)S(1)}, u32[]{:S(2)}, u32[]{:S(2)}) %collective-permute-start.33) | collective-permute-done | bytes 90144 | tf_op jit(solution)/shard_map/ppermute | solution.py:54
  113.0 3.6 %collective-permute-done.32.refs_2_ = bf16[176,256]{1,0:T(8,128)(2,1)S(1)} collective-permute-done((bf16[176,256]{1,0:T(8,128)(2,1)S(1)}, bf16[176,256]{1,0:T(8,128)(2,1)S(1)}, u32[]{:S(2)}, u32[]{:S(2)}) %collective-permute-start.32) | collective-permute-done | bytes 90144 | tf_op jit(solution)/shard_map/ppermute | solution.py:54
  116.6 1.0 collective-permute-done.31.refs_1_
  118.0 0.5 collective-permute-start.35
  118.8 7.7 %collective-permute-start.37 = (bf16[256,256]{1,0:T(8,128)(2,1)S(1)}, bf16[256,256]{1,0:T(8,128)(2,1)S(1)}, u32[]{:S(2)}, u32[]{:S(2)}) collective-permute-start(bf16[256,256]{1,0:T(8,128)(2,1)S(1)} %shard_map.117), channel_id=1, source_target_pairs={{0,64},{1,17},{2,66},{3,19},{4,68},{5,21},{6,70},{7,23},{8,72},{9,... | collective-permute-start | bytes 393224 | tf_op jit(solution)/shard_map/ppermute | solution.py:54
  127.2 3.7 %collective-permute-done.37.c = bf16[256,256]{1,0:T(8,128)(2,1)S(1)} collective-permute-done((bf16[256,256]{1,0:T(8,128)(2,1)S(1)}, bf16[256,256]{1,0:T(8,128)(2,1)S(1)}, u32[]{:S(2)}, u32[]{:S(2)}) %collective-permute-start.37) | collective-permute-done | bytes 131104 | tf_op jit(solution)/shard_map/ppermute | solution.py:54
  130.9 1.4 collective-permute-done.39.d
  132.3 1.2 collective-permute-start.42
  133.5 1.7 %collective-permute-start.41 = (bf16[256,256]{1,0:T(8,128)(2,1)S(1)}, bf16[256,256]{1,0:T(8,128)(2,1)S(1)}, u32[]{:S(2)}, u32[]{:S(2)}) collective-permute-start(bf16[256,256]{1,0:T(8,128)(2,1)S(1)} %shard_map.119.a), channel_id=1, source_target_pairs={{0,4},{1,5},{2,6},{3,7},{4,0},{5,1},{6,2},{7,3},{8,12},{9,13},{10,... | collective-permute-start | bytes 393224 | tf_op jit(solution)/shard_map/ppermute | solution.py:54
  135.2 0.5 collective-permute-start.40
  135.7 1.8 %collective-permute-done.42.d = bf16[256,256]{1,0:T(8,128)(2,1)S(1)} collective-permute-done((bf16[256,256]{1,0:T(8,128)(2,1)S(1)}, bf16[256,256]{1,0:T(8,128)(2,1)S(1)}, u32[]{:S(2)}, u32[]{:S(2)}) %collective-permute-start.42) | collective-permute-done | bytes 131104 | tf_op jit(solution)/shard_map/ppermute | solution.py:54
  137.5 1.7 %collective-permute-done.41.c = bf16[256,256]{1,0:T(8,128)(2,1)S(1)} collective-permute-done((bf16[256,256]{1,0:T(8,128)(2,1)S(1)}, bf16[256,256]{1,0:T(8,128)(2,1)S(1)}, u32[]{:S(2)}, u32[]{:S(2)}) %collective-permute-start.41) | collective-permute-done | bytes 131104 | tf_op jit(solution)/shard_map/ppermute | solution.py:54
  139.6 12.3 %collective-permute-start.43 = (bf16[2,128,256]{2,1,0:T(8,128)(2,1)S(1)}, bf16[2,128,256]{2,1,0:T(8,128)(2,1)S(1)}, u32[]{:S(2)}, u32[]{:S(2)}) collective-permute-start(bf16[2,128,256]{2,1,0:T(8,128)(2,1)S(1)} %shard_map.120.mine), channel_id=1, source_target_pairs={{0,1},{1,0},{2,3},{3,2},{4,5},{5,4},{6,7},{7,6},{8,9},{9,8},{10,11... | collective-permute-start | bytes 393224 | tf_op jit(solution)/shard_map/ppermute | solution.py:36
  151.9 1.0 collective-permute-done.43.other
  152.9 0.7 shard_map.121
  (65 shorter events, 4.7 us)
Async XLA Ops:
  1.7 3.0 %copy-start = (f32[2,3,1408]{2,0,1:T(2,128)S(1)}, f32[2,3,1408]{2,0,1:T(2,128)}, u32[]{:S(2)}) copy-start(f32[2,3,1408]{2,0,1:T(2,128)} %param.13) | copy-start | bytes 101380
  1.7 3.0 %copy-start.1 = (f32[2,3,1408]{2,0,1:T(2,128)S(1)}, f32[2,3,1408]{2,0,1:T(2,128)}, u32[]{:S(2)}) copy-start(f32[2,3,1408]{2,0,1:T(2,128)} %param.14) | copy-start | bytes 101380
  1.7 3.0 %copy-start.2 = (f32[2,1408]{1,0:T(2,128)S(1)}, f32[2,1408]{1,0:T(2,128)}, u32[]{:S(2)}) copy-start(f32[2,1408]{1,0:T(2,128)} %gate_bias.1) | copy-start | bytes 33796
  1.7 3.0 %copy-start.3 = (f32[2,1408]{1,0:T(2,128)S(1)}, f32[2,1408]{1,0:T(2,128)}, u32[]{:S(2)}) copy-start(f32[2,1408]{1,0:T(2,128)} %up_bias.1) | copy-start | bytes 33796
  1.7 11.9 %collective-permute-start.4 = (bf16[2816,256]{1,0:T(8,128)(2,1)S(1)}, bf16[2816,256]{1,0:T(8,128)(2,1)S(1)}, u32[]{:S(2)}, u32[]{:S(2)}) collective-permute-start(bf16[2816,256]{1,0:T(8,128)(2,1)S(1)} %shard_map.96.mine), channel_id=1, source_target_pairs={{0,1},{1,0},{2,3},{3,2},{4,5},{5,4},{6,7},{7,6},{8,9},{9,8},{10,11... | collective-permute-start | bytes 4325384 | tf_op jit(solution)/shard_map/ppermute | solution.py:36
  4.6 8.9 %collective-permute-start.3 = (bf16[4,256,384]{2,1,0:T(8,128)(2,1)S(1)}, bf16[4,256,384]{2,1,0:T(8,128)(2,1)S(1)}, u32[]{:S(2)}, u32[]{:S(2)}) collective-permute-start(bf16[4,256,384]{2,1,0:T(8,128)(2,1)S(1)} %shard_map.94.refs_0_), channel_id=1, source_target_pairs={{0,1},{1,0},{2,3},{3,2},{4,5},{5,4},{6,7},{7,6},{8,9},{9,8},{10,11... | collective-permute-start | bytes 2359304 | tf_op jit(solution)/shard_map/ppermute | solution.py:36
  4.7 6.6 %collective-permute-start.5 = (f32[2,8,1408]{2,1,0:T(8,128)S(1)}, f32[2,8,1408]{2,1,0:T(8,128)S(1)}, u32[]{:S(2)}, u32[]{:S(2)}) collective-permute-start(f32[2,8,1408]{2,1,0:T(8,128)S(1)} %shard_map.98.mine), channel_id=1, source_target_pairs={{0,1},{1,0},{2,3},{3,2},{4,5},{5,4},{6,7},{7,6},{8,9},{9,8},{10,11... | collective-permute-start | bytes 270344 | tf_op jit(solution)/shard_map/ppermute | solution.py:36
  7.2 9.5 %collective-permute-start = (bf16[1232,256]{1,0:T(8,128)(2,1)S(1)}, bf16[1232,256]{1,0:T(8,128)(2,1)S(1)}, u32[]{:S(2)}, u32[]{:S(2)}) collective-permute-start(bf16[1232,256]{1,0:T(8,128)(2,1)S(1)} %get-tuple-element.49), channel_id=1, source_target_pairs={{0,32},{1,9},{2,34},{3,11},{4,36},{5,13},{6,38},{7,15},{8,40},{9,1... | collective-permute-start | bytes 1892360 | tf_op jit(solution)/shard_map/ppermute | solution.py:54
  8.7 17.4 %collective-permute-start.1 = (bf16[1232,256]{1,0:T(8,128)(2,1)S(1)}, bf16[1232,256]{1,0:T(8,128)(2,1)S(1)}, u32[]{:S(2)}, u32[]{:S(2)}) collective-permute-start(bf16[1232,256]{1,0:T(8,128)(2,1)S(1)} %get-tuple-element.50), channel_id=1, source_target_pairs={{0,64},{1,17},{2,66},{3,19},{4,68},{5,21},{6,70},{7,23},{8,72},{9,... | collective-permute-start | bytes 1892360 | tf_op jit(solution)/shard_map/ppermute | solution.py:54
  11.3 17.4 %collective-permute-start.2 = (bf16[1232,256]{1,0:T(8,128)(2,1)S(1)}, bf16[1232,256]{1,0:T(8,128)(2,1)S(1)}, u32[]{:S(2)}, u32[]{:S(2)}) collective-permute-start(bf16[1232,256]{1,0:T(8,128)(2,1)S(1)} %get-tuple-element.51), channel_id=1, source_target_pairs={{0,96},{1,25},{2,98},{3,27},{4,100},{5,29},{6,102},{7,31},{8,104},... | collective-permute-start | bytes 1892360 | tf_op jit(solution)/shard_map/ppermute | solution.py:54
  29.6 4.7 %collective-permute-start.6 = (bf16[184,512]{1,0:T(8,128)(2,1)S(1)}, bf16[184,512]{1,0:T(8,128)(2,1)S(1)}, u32[]{:S(2)}, u32[]{:S(2)}) collective-permute-start(bf16[184,512]{1,0:T(8,128)(2,1)S(1)} %get-tuple-element.70), channel_id=1, source_target_pairs={{0,8},{1,33},{2,10},{3,35},{4,12},{5,37},{6,14},{7,39},{8,0},{9,41... | collective-permute-start | bytes 565256 | tf_op jit(solution)/shard_map/ppermute | solution.py:54
  31.0 8.4 %collective-permute-start.7 = (bf16[184,512]{1,0:T(8,128)(2,1)S(1)}, bf16[184,512]{1,0:T(8,128)(2,1)S(1)}, u32[]{:S(2)}, u32[]{:S(2)}) collective-permute-start(bf16[184,512]{1,0:T(8,128)(2,1)S(1)} %get-tuple-element.71), channel_id=1, source_target_pairs={{0,16},{1,65},{2,18},{3,67},{4,20},{5,69},{6,22},{7,71},{8,24},{9,... | collective-permute-start | bytes 565256 | tf_op jit(solution)/shard_map/ppermute | solution.py:54
  34.3 7.3 %collective-permute-start.8 = (bf16[184,512]{1,0:T(8,128)(2,1)S(1)}, bf16[184,512]{1,0:T(8,128)(2,1)S(1)}, u32[]{:S(2)}, u32[]{:S(2)}) collective-permute-start(bf16[184,512]{1,0:T(8,128)(2,1)S(1)} %get-tuple-element.72), channel_id=1, source_target_pairs={{0,24},{1,97},{2,26},{3,99},{4,28},{5,101},{6,30},{7,103},{8,16},{... | collective-permute-start | bytes 565256 | tf_op jit(solution)/shard_map/ppermute | solution.py:54
  42.2 4.8 %collective-permute-start.11 = (bf16[88,512]{1,0:T(8,128)(2,1)S(1)}, bf16[88,512]{1,0:T(8,128)(2,1)S(1)}, u32[]{:S(2)}, u32[]{:S(2)}) collective-permute-start(bf16[88,512]{1,0:T(8,128)(2,1)S(1)} %shard_map.102.refs_0_), channel_id=1, source_target_pairs={{0,24},{1,97},{2,26},{3,99},{4,28},{5,101},{6,30},{7,103},{8,16},{... | collective-permute-start | bytes 270344 | tf_op jit(solution)/shard_map/ppermute | solution.py:54
  42.3 9.3 %collective-permute-start.12 = (bf16[256,384]{1,0:T(8,128)(2,1)S(1)}, bf16[256,384]{1,0:T(8,128)(2,1)S(1)}, u32[]{:S(2)}, u32[]{:S(2)}) collective-permute-start(bf16[256,384]{1,0:T(8,128)(2,1)S(1)} %get-tuple-element.52), channel_id=1, source_target_pairs={{0,32},{1,9},{2,34},{3,11},{4,36},{5,13},{6,38},{7,15},{8,40},{9,1... | collective-permute-start | bytes 589832 | tf_op jit(solution)/shard_map/ppermute | solution.py:54
  42.4 10.1 %collective-permute-start.14 = (bf16[256,384]{1,0:T(8,128)(2,1)S(1)}, bf16[256,384]{1,0:T(8,128)(2,1)S(1)}, u32[]{:S(2)}, u32[]{:S(2)}) collective-permute-start(bf16[256,384]{1,0:T(8,128)(2,1)S(1)} %get-tuple-element.53), channel_id=1, source_target_pairs={{0,64},{1,17},{2,66},{3,19},{4,68},{5,21},{6,70},{7,23},{8,72},{9,... | collective-permute-start | bytes 589832 | tf_op jit(solution)/shard_map/ppermute | solution.py:54
  43.9 5.6 %collective-permute-start.10 = (bf16[88,512]{1,0:T(8,128)(2,1)S(1)}, bf16[88,512]{1,0:T(8,128)(2,1)S(1)}, u32[]{:S(2)}, u32[]{:S(2)}) collective-permute-start(bf16[88,512]{1,0:T(8,128)(2,1)S(1)} %shard_map.102.refs_0_), channel_id=1, source_target_pairs={{0,16},{1,65},{2,18},{3,67},{4,20},{5,69},{6,22},{7,71},{8,24},{9,... | collective-permute-start | bytes 270344 | tf_op jit(solution)/shard_map/ppermute | solution.py:54
  44.5 7.0 %collective-permute-start.9 = (bf16[88,512]{1,0:T(8,128)(2,1)S(1)}, bf16[88,512]{1,0:T(8,128)(2,1)S(1)}, u32[]{:S(2)}, u32[]{:S(2)}) collective-permute-start(bf16[88,512]{1,0:T(8,128)(2,1)S(1)} %shard_map.102.refs_0_), channel_id=1, source_target_pairs={{0,8},{1,33},{2,10},{3,35},{4,12},{5,37},{6,14},{7,39},{8,0},{9,41... | collective-permute-start | bytes 270344 | tf_op jit(solution)/shard_map/ppermute | solution.py:54
  47.1 9.2 %collective-permute-start.16 = (bf16[256,384]{1,0:T(8,128)(2,1)S(1)}, bf16[256,384]{1,0:T(8,128)(2,1)S(1)}, u32[]{:S(2)}, u32[]{:S(2)}) collective-permute-start(bf16[256,384]{1,0:T(8,128)(2,1)S(1)} %get-tuple-element.54), channel_id=1, source_target_pairs={{0,96},{1,25},{2,98},{3,27},{4,100},{5,29},{6,102},{7,31},{8,104},... | collective-permute-start | bytes 589832 | tf_op jit(solution)/shard_map/ppermute | solution.py:54
  52.0 5.3 %collective-permute-start.13 = (bf16[256,512]{1,0:T(8,128)(2,1)S(1)}, bf16[256,512]{1,0:T(8,128)(2,1)S(1)}, u32[]{:S(2)}, u32[]{:S(2)}) collective-permute-start(bf16[256,512]{1,0:T(8,128)(2,1)S(1)} %shard_map.105), channel_id=1, source_target_pairs={{0,32},{1,9},{2,34},{3,11},{4,36},{5,13},{6,38},{7,15},{8,40},{9,1... | collective-permute-start | bytes 786440 | tf_op jit(solution)/shard_map/ppermute | solution.py:54
  52.8 9.7 %collective-permute-start.15 = (bf16[256,512]{1,0:T(8,128)(2,1)S(1)}, bf16[256,512]{1,0:T(8,128)(2,1)S(1)}, u32[]{:S(2)}, u32[]{:S(2)}) collective-permute-start(bf16[256,512]{1,0:T(8,128)(2,1)S(1)} %shard_map.106), channel_id=1, source_target_pairs={{0,64},{1,17},{2,66},{3,19},{4,68},{5,21},{6,70},{7,23},{8,72},{9,... | collective-permute-start | bytes 786440 | tf_op jit(solution)/shard_map/ppermute | solution.py:54
  56.5 9.0 %collective-permute-start.17 = (bf16[256,512]{1,0:T(8,128)(2,1)S(1)}, bf16[256,512]{1,0:T(8,128)(2,1)S(1)}, u32[]{:S(2)}, u32[]{:S(2)}) collective-permute-start(bf16[256,512]{1,0:T(8,128)(2,1)S(1)} %shard_map.107), channel_id=1, source_target_pairs={{0,96},{1,25},{2,98},{3,27},{4,100},{5,29},{6,102},{7,31},{8,104},... | collective-permute-start | bytes 786440 | tf_op jit(solution)/shard_map/ppermute | solution.py:54
  65.6 8.8 %collective-permute-start.18 = (bf16[256,256]{1,0:T(8,128)(2,1)S(1)}, bf16[256,256]{1,0:T(8,128)(2,1)S(1)}, u32[]{:S(2)}, u32[]{:S(2)}) collective-permute-start(bf16[256,256]{1,0:T(8,128)(2,1)S(1)} %get-tuple-element.74), channel_id=1, source_target_pairs={{0,1},{1,0},{2,3},{3,2},{4,5},{5,4},{6,7},{7,6},{8,9},{9,8},{10,11... | collective-permute-start | bytes 393224 | tf_op jit(solution)/shard_map/ppermute | solution.py:36
  70.6 27.8 %collective-permute-start.22 = (bf16[1408,256]{1,0:T(8,128)(2,1)S(1)}, bf16[1408,256]{1,0:T(8,128)(2,1)S(1)}, u32[]{:S(2)}, u32[]{:S(2)}) collective-permute-start(bf16[1408,256]{1,0:T(8,128)(2,1)S(1)} %get-tuple-element.76), channel_id=1, source_target_pairs={{0,32},{1,9},{2,34},{3,11},{4,36},{5,13},{6,38},{7,15},{8,40},{9,1... | collective-permute-start | bytes 2162696 | tf_op jit(solution)/shard_map/ppermute | solution.py:54
  71.0 27.3 %collective-permute-start.23 = (bf16[1408,256]{1,0:T(8,128)(2,1)S(1)}, bf16[1408,256]{1,0:T(8,128)(2,1)S(1)}, u32[]{:S(2)}, u32[]{:S(2)}) collective-permute-start(bf16[1408,256]{1,0:T(8,128)(2,1)S(1)} %get-tuple-element.77), channel_id=1, source_target_pairs={{0,64},{1,17},{2,66},{3,19},{4,68},{5,21},{6,70},{7,23},{8,72},{9,... | collective-permute-start | bytes 2162696 | tf_op jit(solution)/shard_map/ppermute | solution.py:54
  72.2 26.1 %collective-permute-start.24 = (bf16[1408,256]{1,0:T(8,128)(2,1)S(1)}, bf16[1408,256]{1,0:T(8,128)(2,1)S(1)}, u32[]{:S(2)}, u32[]{:S(2)}) collective-permute-start(bf16[1408,256]{1,0:T(8,128)(2,1)S(1)} %get-tuple-element.78), channel_id=1, source_target_pairs={{0,96},{1,25},{2,98},{3,27},{4,100},{5,29},{6,102},{7,31},{8,104},... | collective-permute-start | bytes 2162696 | tf_op jit(solution)/shard_map/ppermute | solution.py:54
  74.4 12.3 %copy-start.4 = (f32[2,256]{1,0:T(2,128)S(1)}, f32[2,256]{1,0:T(2,128)}, u32[]{:S(2)}) copy-start(f32[2,256]{1,0:T(2,128)} %gain.3) | copy-start | bytes 6148
  74.5 8.1 %collective-permute-start.21 = (bf16[256,256]{1,0:T(8,128)(2,1)S(1)}, bf16[256,256]{1,0:T(8,128)(2,1)S(1)}, u32[]{:S(2)}, u32[]{:S(2)}) collective-permute-start(bf16[256,256]{1,0:T(8,128)(2,1)S(1)} %shard_map.109.a), channel_id=1, source_target_pairs={{0,6},{1,7},{2,4},{3,5},{4,2},{5,3},{6,0},{7,1},{8,14},{9,15},{10,... | collective-permute-start | bytes 393224 | tf_op jit(solution)/shard_map/ppermute | solution.py:54
  77.0 5.6 %collective-permute-start.20 = (bf16[256,256]{1,0:T(8,128)(2,1)S(1)}, bf16[256,256]{1,0:T(8,128)(2,1)S(1)}, u32[]{:S(2)}, u32[]{:S(2)}) collective-permute-start(bf16[256,256]{1,0:T(8,128)(2,1)S(1)} %shard_map.109.a), channel_id=1, source_target_pairs={{0,4},{1,5},{2,6},{3,7},{4,0},{5,1},{6,2},{7,3},{8,12},{9,13},{10,... | collective-permute-start | bytes 393224 | tf_op jit(solution)/shard_map/ppermute | solution.py:54
  82.6 4.1 %collective-permute-start.19 = (bf16[256,256]{1,0:T(8,128)(2,1)S(1)}, bf16[256,256]{1,0:T(8,128)(2,1)S(1)}, u32[]{:S(2)}, u32[]{:S(2)}) collective-permute-start(bf16[256,256]{1,0:T(8,128)(2,1)S(1)} %shard_map.109.a), channel_id=1, source_target_pairs={{0,2},{1,3},{2,0},{3,1},{4,6},{5,7},{6,4},{7,5},{8,10},{9,11},{10,... | collective-permute-start | bytes 393224 | tf_op jit(solution)/shard_map/ppermute | solution.py:54
  87.0 7.5 %collective-permute-start.27 = (bf16[264,256]{1,0:T(8,128)(2,1)S(1)}, bf16[264,256]{1,0:T(8,128)(2,1)S(1)}, u32[]{:S(2)}, u32[]{:S(2)}) collective-permute-start(bf16[264,256]{1,0:T(8,128)(2,1)S(1)} %get-tuple-element.79.refs_1_), channel_id=1, source_target_pairs={{0,96},{1,25},{2,98},{3,27},{4,100},{5,29},{6,102},{7,31},{8,104},... | collective-permute-start | bytes 405512 | tf_op jit(solution)/shard_map/ppermute | solution.py:54
  87.5 7.3 %collective-permute-start.26 = (bf16[264,256]{1,0:T(8,128)(2,1)S(1)}, bf16[264,256]{1,0:T(8,128)(2,1)S(1)}, u32[]{:S(2)}, u32[]{:S(2)}) collective-permute-start(bf16[264,256]{1,0:T(8,128)(2,1)S(1)} %get-tuple-element.79.refs_1_), channel_id=1, source_target_pairs={{0,64},{1,17},{2,66},{3,19},{4,68},{5,21},{6,70},{7,23},{8,72},{9,... | collective-permute-start | bytes 405512 | tf_op jit(solution)/shard_map/ppermute | solution.py:54
  94.5 3.9 %collective-permute-start.25 = (bf16[264,256]{1,0:T(8,128)(2,1)S(1)}, bf16[264,256]{1,0:T(8,128)(2,1)S(1)}, u32[]{:S(2)}, u32[]{:S(2)}) collective-permute-start(bf16[264,256]{1,0:T(8,128)(2,1)S(1)} %get-tuple-element.79.refs_1_), channel_id=1, source_target_pairs={{0,32},{1,9},{2,34},{3,11},{4,36},{5,13},{6,38},{7,15},{8,40},{9,1... | collective-permute-start | bytes 405512 | tf_op jit(solution)/shard_map/ppermute | solution.py:54
  99.3 7.5 %collective-permute-start.28 = (bf16[360,256]{1,0:T(8,128)(2,1)S(1)}, bf16[360,256]{1,0:T(8,128)(2,1)S(1)}, u32[]{:S(2)}, u32[]{:S(2)}) collective-permute-start(bf16[360,256]{1,0:T(8,128)(2,1)S(1)} %get-tuple-element.83), channel_id=1, source_target_pairs={{0,8},{1,33},{2,10},{3,35},{4,12},{5,37},{6,14},{7,39},{8,0},{9,41... | collective-permute-start | bytes 552968 | tf_op jit(solution)/shard_map/ppermute | solution.py:54
  99.3 7.7 %collective-permute-start.29 = (bf16[360,256]{1,0:T(8,128)(2,1)S(1)}, bf16[360,256]{1,0:T(8,128)(2,1)S(1)}, u32[]{:S(2)}, u32[]{:S(2)}) collective-permute-start(bf16[360,256]{1,0:T(8,128)(2,1)S(1)} %get-tuple-element.84), channel_id=1, source_target_pairs={{0,16},{1,65},{2,18},{3,67},{4,20},{5,69},{6,22},{7,71},{8,24},{9,... | collective-permute-start | bytes 552968 | tf_op jit(solution)/shard_map/ppermute | solution.py:54
  100.5 6.9 %collective-permute-start.30 = (bf16[360,256]{1,0:T(8,128)(2,1)S(1)}, bf16[360,256]{1,0:T(8,128)(2,1)S(1)}, u32[]{:S(2)}, u32[]{:S(2)}) collective-permute-start(bf16[360,256]{1,0:T(8,128)(2,1)S(1)} %get-tuple-element.85), channel_id=1, source_target_pairs={{0,24},{1,97},{2,26},{3,99},{4,28},{5,101},{6,30},{7,103},{8,16},{... | collective-permute-start | bytes 552968 | tf_op jit(solution)/shard_map/ppermute | solution.py:54
  103.2 14.5 %collective-permute-start.34 = (bf16[256,768]{1,0:T(8,128)(2,1)S(1)}, bf16[256,768]{1,0:T(8,128)(2,1)S(1)}, u32[]{:S(2)}, u32[]{:S(2)}) collective-permute-start(bf16[256,768]{1,0:T(8,128)(2,1)S(1)} %get-tuple-element.86), channel_id=1, source_target_pairs={{0,32},{1,9},{2,34},{3,11},{4,36},{5,13},{6,38},{7,15},{8,40},{9,1... | collective-permute-start | bytes 1179656 | tf_op jit(solution)/shard_map/ppermute | solution.py:54
  103.2 15.3 %collective-permute-start.36 = (bf16[256,768]{1,0:T(8,128)(2,1)S(1)}, bf16[256,768]{1,0:T(8,128)(2,1)S(1)}, u32[]{:S(2)}, u32[]{:S(2)}) collective-permute-start(bf16[256,768]{1,0:T(8,128)(2,1)S(1)} %get-tuple-element.87), channel_id=1, source_target_pairs={{0,64},{1,17},{2,66},{3,19},{4,68},{5,21},{6,70},{7,23},{8,72},{9,... | collective-permute-start | bytes 1179656 | tf_op jit(solution)/shard_map/ppermute | solution.py:54
  106.8 19.7 %collective-permute-start.38 = (bf16[256,768]{1,0:T(8,128)(2,1)S(1)}, bf16[256,768]{1,0:T(8,128)(2,1)S(1)}, u32[]{:S(2)}, u32[]{:S(2)}) collective-permute-start(bf16[256,768]{1,0:T(8,128)(2,1)S(1)} %get-tuple-element.88), channel_id=1, source_target_pairs={{0,96},{1,25},{2,98},{3,27},{4,100},{5,29},{6,102},{7,31},{8,104},... | collective-permute-start | bytes 1179656 | tf_op jit(solution)/shard_map/ppermute | solution.py:54
  107.9 5.0 %collective-permute-start.33 = (bf16[176,256]{1,0:T(8,128)(2,1)S(1)}, bf16[176,256]{1,0:T(8,128)(2,1)S(1)}, u32[]{:S(2)}, u32[]{:S(2)}) collective-permute-start(bf16[176,256]{1,0:T(8,128)(2,1)S(1)} %shard_map.113.refs_0_), channel_id=1, source_target_pairs={{0,24},{1,97},{2,26},{3,99},{4,28},{5,101},{6,30},{7,103},{8,16},{... | collective-permute-start | bytes 270344 | tf_op jit(solution)/shard_map/ppermute | solution.py:54
  110.8 5.9 %collective-permute-start.32 = (bf16[176,256]{1,0:T(8,128)(2,1)S(1)}, bf16[176,256]{1,0:T(8,128)(2,1)S(1)}, u32[]{:S(2)}, u32[]{:S(2)}) collective-permute-start(bf16[176,256]{1,0:T(8,128)(2,1)S(1)} %shard_map.113.refs_0_), channel_id=1, source_target_pairs={{0,16},{1,65},{2,18},{3,67},{4,20},{5,69},{6,22},{7,71},{8,24},{9,... | collective-permute-start | bytes 270344 | tf_op jit(solution)/shard_map/ppermute | solution.py:54
  113.0 4.6 %collective-permute-start.31 = (bf16[176,256]{1,0:T(8,128)(2,1)S(1)}, bf16[176,256]{1,0:T(8,128)(2,1)S(1)}, u32[]{:S(2)}, u32[]{:S(2)}) collective-permute-start(bf16[176,256]{1,0:T(8,128)(2,1)S(1)} %shard_map.113.refs_0_), channel_id=1, source_target_pairs={{0,8},{1,33},{2,10},{3,35},{4,12},{5,37},{6,14},{7,39},{8,0},{9,41... | collective-permute-start | bytes 270344 | tf_op jit(solution)/shard_map/ppermute | solution.py:54
  118.0 9.2 %collective-permute-start.35 = (bf16[256,256]{1,0:T(8,128)(2,1)S(1)}, bf16[256,256]{1,0:T(8,128)(2,1)S(1)}, u32[]{:S(2)}, u32[]{:S(2)}) collective-permute-start(bf16[256,256]{1,0:T(8,128)(2,1)S(1)} %shard_map.116), channel_id=1, source_target_pairs={{0,32},{1,9},{2,34},{3,11},{4,36},{5,13},{6,38},{7,15},{8,40},{9,1... | collective-permute-start | bytes 393224 | tf_op jit(solution)/shard_map/ppermute | solution.py:54
  118.8 12.1 %collective-permute-start.37 = (bf16[256,256]{1,0:T(8,128)(2,1)S(1)}, bf16[256,256]{1,0:T(8,128)(2,1)S(1)}, u32[]{:S(2)}, u32[]{:S(2)}) collective-permute-start(bf16[256,256]{1,0:T(8,128)(2,1)S(1)} %shard_map.117), channel_id=1, source_target_pairs={{0,64},{1,17},{2,66},{3,19},{4,68},{5,21},{6,70},{7,23},{8,72},{9,... | collective-permute-start | bytes 393224 | tf_op jit(solution)/shard_map/ppermute | solution.py:54
  126.8 5.5 %collective-permute-start.39 = (bf16[256,256]{1,0:T(8,128)(2,1)S(1)}, bf16[256,256]{1,0:T(8,128)(2,1)S(1)}, u32[]{:S(2)}, u32[]{:S(2)}) collective-permute-start(bf16[256,256]{1,0:T(8,128)(2,1)S(1)} %shard_map.118), channel_id=1, source_target_pairs={{0,96},{1,25},{2,98},{3,27},{4,100},{5,29},{6,102},{7,31},{8,104},... | collective-permute-start | bytes 393224 | tf_op jit(solution)/shard_map/ppermute | solution.py:54
  132.3 5.1 %collective-permute-start.42 = (bf16[256,256]{1,0:T(8,128)(2,1)S(1)}, bf16[256,256]{1,0:T(8,128)(2,1)S(1)}, u32[]{:S(2)}, u32[]{:S(2)}) collective-permute-start(bf16[256,256]{1,0:T(8,128)(2,1)S(1)} %shard_map.119.a), channel_id=1, source_target_pairs={{0,6},{1,7},{2,4},{3,5},{4,2},{5,3},{6,0},{7,1},{8,14},{9,15},{10,... | collective-permute-start | bytes 393224 | tf_op jit(solution)/shard_map/ppermute | solution.py:54
  133.5 5.6 %collective-permute-start.41 = (bf16[256,256]{1,0:T(8,128)(2,1)S(1)}, bf16[256,256]{1,0:T(8,128)(2,1)S(1)}, u32[]{:S(2)}, u32[]{:S(2)}) collective-permute-start(bf16[256,256]{1,0:T(8,128)(2,1)S(1)} %shard_map.119.a), channel_id=1, source_target_pairs={{0,4},{1,5},{2,6},{3,7},{4,0},{5,1},{6,2},{7,3},{8,12},{9,13},{10,... | collective-permute-start | bytes 393224 | tf_op jit(solution)/shard_map/ppermute | solution.py:54
  135.2 4.2 %collective-permute-start.40 = (bf16[256,256]{1,0:T(8,128)(2,1)S(1)}, bf16[256,256]{1,0:T(8,128)(2,1)S(1)}, u32[]{:S(2)}, u32[]{:S(2)}) collective-permute-start(bf16[256,256]{1,0:T(8,128)(2,1)S(1)} %shard_map.119.a), channel_id=1, source_target_pairs={{0,2},{1,3},{2,0},{3,1},{4,6},{5,7},{6,4},{7,5},{8,10},{9,11},{10,... | collective-permute-start | bytes 393224 | tf_op jit(solution)/shard_map/ppermute | solution.py:54
  139.6 13.3 %collective-permute-start.43 = (bf16[2,128,256]{2,1,0:T(8,128)(2,1)S(1)}, bf16[2,128,256]{2,1,0:T(8,128)(2,1)S(1)}, u32[]{:S(2)}, u32[]{:S(2)}) collective-permute-start(bf16[2,128,256]{2,1,0:T(8,128)(2,1)S(1)} %shard_map.120.mine), channel_id=1, source_target_pairs={{0,1},{1,0},{2,3},{3,2},{4,5},{5,4},{6,7},{7,6},{8,9},{9,8},{10,11... | collective-permute-start | bytes 393224 | tf_op jit(solution)/shard_map/ppermute | solution.py:36
